TPU v7x, 128 devices: a whole 4x4x4 slice. The times are simulated.
128 devices in a mesh: sp: 16 (over z, x), tp: 8 (over y, core).
Axes of the slice: x: 4, y: 4, z: 4, core: 2. Of those that a mesh axis runs over, the one named last changes fastest.
Arguments:
- activation_sequence: bfloat16 [32768, 2, 2048], P(('sp', 'tp')), may hold values from -6 to 6
- rms_multiplier_vector: bfloat16 [2048], replicated, may hold values from 0.099609375 to 1.8984375
- linear_memory_source_matrix: bfloat16 [2048, 1024], P('sp', 'tp'), may hold values from -0.125 to 0.125
- linear_memory_exit_matrix: bfloat16 [2048, 1024], P('sp', 'tp'), may hold values from -0.125 to 0.125
- filter_exit_mask_matrix: bfloat16 [2048, 1024], P('sp', 'tp'), may hold values from -0.125 to 0.125
- filter_entry_mask_matrix: bfloat16 [2048, 1024], P('sp', 'tp'), may hold values from -0.125 to 0.125
- filter_source_matrix: bfloat16 [2048, 1024], P('sp', 'tp'), may hold values from -0.125 to 0.125
- memory_prefilter_taps: bfloat16 [4, 1024], P(None, 'tp'), may hold values from -3 to 3
- filter_taps_depthwise: bfloat16 [3, 1024], P(None, 'tp'), may hold values from -3.5 to 3.5
- fading_mask_diagonal_tiles: bfloat16 [2, 8, 128, 128], P(None, 'tp'), may hold values from -0.5 to 0.5
- entry_mask_diagonal_tiles: bfloat16 [2, 8, 128, 128], P(None, 'tp'), may hold values from -0.5 to 0.5
- fading_speed_per_channel: float32 [2, 1024], P(None, 'tp'), may hold values from 0 to 0.012
- speed_multiplier: float32 [32768], P('sp'), may hold values from 0.28 to 3.5
- jump_per_position: float32 [32768], P('sp'), may hold values from -2.1 to 0
- boundary_hidden_vectors: float32 [2, 2, 1024], P(None, None, 'tp'), may hold values from -6 to 6
- final_mixing_matrix: bfloat16 [2, 1024, 2048], P(None, None, ('sp', 'tp')), may hold values from -0.125 to 0.125
Outputs:
- mixed: bfloat16 [32768, 2, 2048], P(('sp', 'tp'))
All inputs are finite; a program needn't handle non-finite values.
Results may differ from a plain program's by a relative error of at most 0.0084.
Values may be sent and summed in bfloat16 or wider, within the bound.
A program may use at most 192 MiB of HBM per device.

v0:
```python
import jax
import jax.numpy as jnp
from jax import lax
from jax.sharding import PartitionSpec as P

epsilon = 1e-06
decay_factor_scale = 8.0


def sent_to_all(x, axis):
    copies = jnp.broadcast_to(x, (lax.axis_size(axis), *x.shape))
    return lax.all_to_all(copies, axis, split_axis=0, concat_axis=0, tiled=True)


def in_order(parts, dim):
    parts = jnp.moveaxis(parts, 0, dim)
    lengths = parts.shape
    return parts.reshape(*lengths[:dim], lengths[dim] * lengths[dim + 1], *lengths[dim + 2 :])


def gathered_copies(x, axis, dim):
    parts = sent_to_all(x, axis)
    return in_order(parts, dim)


def on_gathered_pieces(x, axis, dim, work, out_dim):
    extent = x.shape[dim]
    pieces = jnp.split(x, 2, axis=dim) if extent % 2 == 0 else [x]
    first = jnp.arange(lax.axis_size(axis)) * extent
    parts = [lax.all_gather(share, axis) for share in pieces]
    made = [jax.vmap(work)(b, first + k * (extent // len(pieces))) for k, b in enumerate(parts)]
    return in_order(jnp.concatenate(made, axis=out_dim + 1), out_dim)


def shifted(value, axis, steps):
    count = lax.axis_size(axis)
    first, last = (max(0, -steps), min(count, count - steps))
    return lax.ppermute(value, axis, [(source, source + steps) for source in range(first, last)])


def combine(earlier, later):
    return (earlier[0] * later[0], later[0] * earlier[1] + later[1])


def advance(state, item):
    return (item[0] * state + item[1], state)


def body(
    activation_sequence,
    rms_multiplier_vector,
    linear_memory_source_matrix,
    linear_memory_exit_matrix,
    filter_exit_mask_matrix,
    filter_entry_mask_matrix,
    filter_source_matrix,
    memory_prefilter_taps,
    filter_taps_depthwise,
    fading_mask_diagonal_tiles,
    entry_mask_diagonal_tiles,
    fading_speed_per_channel,
    speed_multiplier,
    jump_per_position,
    boundary_hidden_vectors,
    final_mixing_matrix,
):
    batch = activation_sequence.shape[1]
    widened = activation_sequence.reshape(-1, activation_sequence.shape[2]).astype(jnp.float32)
    normed = (
        widened
        * lax.rsqrt(jnp.mean(widened * widened, axis=-1, keepdims=True) + epsilon)
        * rms_multiplier_vector.astype(jnp.float32)
    ).astype(jnp.bfloat16)
    local_weights = jnp.concatenate(
        [
            linear_memory_source_matrix,
            linear_memory_exit_matrix,
            filter_exit_mask_matrix,
            filter_entry_mask_matrix,
            filter_source_matrix,
        ],
        axis=1,
    )
    in_weights = gathered_copies(local_weights, "sp", 0)

    def project(piece, start):
        return jnp.dot(piece, in_weights, preferred_element_type=jnp.float32).astype(jnp.bfloat16)

    projected = on_gathered_pieces(normed, "tp", 0, project, 0)
    channels = in_weights.shape[1] // 5
    length = projected.shape[0] // batch
    width = batch * channels

    def role(number):
        return projected[:, number * channels : (number + 1) * channels].reshape(length, width)

    rec_in = role(0)
    rec_gate = role(1)
    conv_out = role(2)
    shaken = (role(3).astype(jnp.float32) * role(4).astype(jnp.float32)).astype(jnp.bfloat16)
    joined = jnp.concatenate([rec_in, shaken], axis=1)
    before = shifted(joined[length - 2 :], "sp", 1)
    after = shifted(joined[:1], "sp", -1)
    padded = jnp.concatenate([before, joined, after], axis=0).astype(jnp.float32)
    rec_taps = jnp.tile(memory_prefilter_taps.astype(jnp.float32), (1, batch))
    conv_taps = jnp.tile(filter_taps_depthwise.astype(jnp.float32), (1, batch))
    rec_conv = jnp.zeros((length, width), jnp.float32)
    for offset in range(rec_taps.shape[0]):
        rec_conv = rec_conv + rec_taps[offset] * padded[offset : offset + length, :width]
    rec_conv = rec_conv.astype(jnp.bfloat16)
    short = jnp.zeros((length, width), jnp.float32)
    for offset in range(conv_taps.shape[0]):
        short = short + conv_taps[offset] * padded[offset + 1 : offset + 1 + length, width:]
    conv_y = (conv_out.astype(jnp.float32) * short).astype(jnp.bfloat16)
    block_count = fading_mask_diagonal_tiles.shape[1]
    identity = jnp.eye(block_count, dtype=jnp.bfloat16)
    fading_dense = jnp.einsum("knde,nm->kndme", fading_mask_diagonal_tiles, identity).reshape(
        2, channels, channels
    )
    entry_dense = jnp.einsum("knde,nm->kndme", entry_mask_diagonal_tiles, identity).reshape(
        2, channels, channels
    )
    flat_conv = rec_conv.reshape(length * batch, channels)
    recurrence_preactivation = jnp.einsum(
        "rc,kce->kre", flat_conv, fading_dense, preferred_element_type=jnp.float32
    ).reshape(2, length, width)
    pre_i = jnp.einsum(
        "rc,kce->kre", flat_conv, entry_dense, preferred_element_type=jnp.float32
    ).reshape(2, length, width)
    widened_conv = rec_conv.astype(jnp.float32)
    speeds = jnp.tile(fading_speed_per_channel, (1, batch))
    tempo_column = speed_multiplier[:, None]
    jump_vertical_vector = jump_per_position[:, None]
    boundary = boundary_hidden_vectors.reshape(2, width)
    cumulative = []
    totals = []
    for scan_direction in range(2):
        log_decay = (
            -decay_factor_scale
            * jax.nn.sigmoid(recurrence_preactivation[scan_direction])
            * speeds[scan_direction]
            * tempo_column
            + jump_vertical_vector
        )
        decay = jnp.exp(log_decay)
        drive = (
            jnp.sqrt(-jnp.expm1(2.0 * log_decay))
            * jax.nn.sigmoid(pre_i[scan_direction])
            * widened_conv
        )
        acum, bcum = lax.associative_scan(
            combine, (decay, drive), axis=0, reverse=scan_direction == 1
        )
        cumulative.append((acum, bcum))
        edge = length - 1 if scan_direction == 0 else 0
        totals.append((acum[edge], bcum[edge]))
    packed = jnp.stack([totals[0][0], totals[0][1], totals[1][0], totals[1][1]])[None]
    every = gathered_copies(packed, "sp", 0)
    _, forward_in = lax.scan(advance, boundary[0], (every[:, 0], every[:, 1]))
    _, backward_in = lax.scan(advance, boundary[1], (every[:, 2], every[:, 3]), reverse=True)
    position = lax.axis_index("sp")
    entering = [
        lax.dynamic_index_in_dim(forward_in, position, 0, keepdims=False),
        lax.dynamic_index_in_dim(backward_in, position, 0, keepdims=False),
    ]
    states = (
        cumulative[0][1]
        + cumulative[0][0] * entering[0][None]
        + cumulative[1][1]
        + cumulative[1][0] * entering[1][None]
    )
    rec_out = (states * jax.nn.gelu(rec_gate.astype(jnp.float32))).astype(jnp.bfloat16)
    outputs = jnp.stack([rec_out, conv_y])
    groups = lax.axis_size("tp")
    own_rows = length // groups
    sliced = lax.all_to_all(final_mixing_matrix, "tp", split_axis=1, concat_axis=2, tiled=True)
    own_weight = lax.all_gather(sliced, "sp", axis=2, tiled=True)
    part_rows = outputs.reshape(2, own_rows * lax.axis_size("tp"), batch, channels)
    return lax.psum_scatter(
        jnp.einsum("klbc,kcd->lbd", part_rows, own_weight, preferred_element_type=jnp.float32),
        "tp",
        scatter_dimension=0,
        tiled=True,
    ).astype(jnp.bfloat16)


def solution(mesh):
    return jax.shard_map(
        body,
        mesh=mesh,
        in_specs=(
            P(("sp", "tp"), None, None),
            P(),
            P("sp", "tp"),
            P("sp", "tp"),
            P("sp", "tp"),
            P("sp", "tp"),
            P("sp", "tp"),
            P(None, "tp"),
            P(None, "tp"),
            P(None, "tp", None, None),
            P(None, "tp", None, None),
            P(None, "tp"),
            P("sp"),
            P("sp"),
            P(None, None, "tp"),
            P(None, None, ("sp", "tp")),
        ),
        out_specs=P(("sp", "tp"), None, None),
        check_vma=False,
    )
```

profile of v0, /device:TPU:1, one launch (start us, length us, event | category | flops | bytes accessed | tf_op | source)
XLA Modules:
  0.0 734.4 jit_solution(12411368137572185214)
XLA Ops:
  7.4 4.0 multiply_reduce_fusion
  21.1 8.6 %all-to-all-start = ((bf16[16,128,640]{2,1,0:T(8,128)(2,1)}), bf16[16,128,640]{2,1,0:T(8,128)(2,1)S(1)}, u32[]{:S(2)}, u32[]{:S(2)}) async-start(bf16[16,128,640]{2,1,0:T(8,128)(2,1)} %broadcast_in_dim.26), calls=%async_computation | async-start | bytes 5242880 | tf_op jit(solution)/shard_map/all_to_all | solution.py:12
  31.3 37.4 %all-to-all-done = bf16[16,128,640]{2,1,0:T(8,128)(2,1)S(1)} async-done(((bf16[16,128,640]{2,1,0:T(8,128)(2,1)}), bf16[16,128,640]{2,1,0:T(8,128)(2,1)S(1)}, u32[]{:S(2)}, u32[]{:S(2)}) %all-to-all-start) | async-done | bytes 2621472 | tf_op jit(solution)/shard_map/all_to_all | solution.py:12
  68.7 6.8 all-to-all-start.2
  75.6 9.9 %convolution_convert_fusion.1 = bf16[8,256,640]{2,1,0:T(8,128)(2,1)S(1)} fusion(bf16[8,256,2048]{2,1,0:T(8,128)(2,1)} %bitcast.132, bf16[2048,640,1]{1,0,2:T(8,128)(2,1)} %bitcast.114), kind=kOutput, calls=%fused_computation.62 | convolution fusion | flops 5370019840 | bytes 13631488 | tf_op jit(solution)/shard_map/vmap()/dot_general | solution.py:87
  85.5 37.9 %all-gather.10.cloned.1.call-done = bf16[2048,2048]{1,0:T(8,128)(2,1)} async-done(((bf16[256,2048]{1,0:T(8,128)(2,1)}), bf16[2048,2048]{1,0:T(8,128)(2,1)}) %all-gather.10.cloned.1.call-update) | async-done | bytes 8388624 | tf_op jit(solution)/shard_map/all_gather | solution.py:30
  123.4 9.9 %convolution_convert_fusion = bf16[8,256,640]{2,1,0:T(8,128)(2,1)S(1)} fusion(bf16[8,256,2048]{2,1,0:T(8,128)(2,1)} %bitcast.133, bf16[2048,640,1]{1,0,2:T(8,128)(2,1)} %bitcast.115), kind=kOutput, calls=%fused_computation.61 | convolution fusion | flops 5370019840 | bytes 13631488 | tf_op jit(solution)/shard_map/vmap()/dot_general | solution.py:87
  148.5 9.5 %concatenate.136 = bf16[2051,512]{1,0:T(8,128)(2,1)S(1)} concatenate(bf16[2,512]{1,0:T(2,128)(2,1)S(1)} %collective-permute-done, bf16[2048,512]{1,0:T(8,128)(2,1)} %copy-done.12, bf16[1,512]{1,0:T(2,128)(2,1)S(1)} %collective-permute-done.1), dimensions={0} | concatenate | bytes 4200448 | tf_op jit(solution)/shard_map/concatenate | solution.py:104
  180.0 7.0 convert_multiply_fusion.1
  189.0 6.3 slice.913
  195.3 6.2 slice.835
  201.6 6.3 slice.834
  209.1 6.3 slice.837
  215.4 6.2 slice.833
  221.6 6.3 slice.832
  231.9 3.7 slice.911
  235.6 3.6 slice.841
  239.2 3.7 slice.840
  276.2 5.1 slice.993
  281.3 6.3 slice.943
  287.6 6.2 slice.941
  294.4 3.5 slice.1050
  297.9 3.5 slice.1000
  301.4 3.5 slice.998
  304.9 8.9 %slice.942 = f32[1024,256]{1,0:T(8,128)} reverse(f32[1024,256]{1,0:T(8,128)} %slice.941), dimensions={0} | reverse | bytes 2097152 | tf_op jit(solution)/shard_map/slice | solution.py:151
  313.8 5.1 slice.944
  319.0 8.9 %slice.999 = f32[1024,256]{1,0:T(8,128)} reverse(f32[1024,256]{1,0:T(8,128)} %slice.998), dimensions={0} | reverse | bytes 2097152 | tf_op jit(solution)/shard_map/slice | solution.py:151
  327.8 5.4 slice.1001
  373.0 5.4 slice.994
  378.4 5.5 slice.1051
  391.5 4.6 pad.309
  402.8 4.2 pad.310
  407.0 4.9 pad.288
  412.0 8.8 %pad.289 = f32[2048,256]{1,0:T(8,128)} pad(f32[1024,256]{1,0:T(8,128)} %add.582, f32[]{:T(128)} %constant.72.clone.1), padding=1_0_1x0_0_0 | pad | bytes 3145732 | tf_op jit(solution)/shard_map/pad | solution.py:151
  422.2 4.8 pad.311
  438.6 4.6 pad.331
  450.0 4.2 pad.332
  454.2 4.8 pad.354
  458.9 8.6 %pad.355 = f32[2048,256]{1,0:T(8,128)} pad(f32[1024,256]{1,0:T(8,128)} %add.639, f32[]{:T(128)} %constant.72.clone.1), padding=1_0_1x0_0_0 | pad | bytes 3145732 | tf_op jit(solution)/shard_map/pad | solution.py:151
  468.2 4.9 pad.333
  474.5 8.3 %all-to-all-start.1 = ((f32[16,1,4,256]{3,2,1,0:T(4,128)}), f32[16,1,4,256]{3,2,1,0:T(4,128)S(1)}, u32[]{:S(2)}, u32[]{:S(2)}) async-start(f32[16,1,4,256]{3,2,1,0:T(4,128)} %broadcast_in_dim.27), calls=%async_computation.1 | async-start | bytes 131072 | tf_op jit(solution)/shard_map/all_to_all | solution.py:12
  487.3 3.9 add.641
  495.9 10.3 %rev.8 = f32[2048,256]{1,0:T(8,128)} reverse(f32[2048,256]{1,0:T(8,128)S(1)} %copy-done.9), dimensions={0} | reverse | bytes 4194304 | tf_op jit(solution)/shard_map/rev | solution.py:151
  506.3 16.8 %rev.9 = f32[2048,256]{1,0:T(8,128)} reverse(f32[2048,256]{1,0:T(8,128)} %add.608), dimensions={0} | reverse | bytes 4194304 | tf_op jit(solution)/shard_map/rev | solution.py:151
  526.4 6.8 fusion.8
  535.4 13.6 %convolution_bitcast_fusion = f32[2048,2,2048]{2,0,1:T(8,128)} fusion(bf16[1,2048,2,128]{3,1,0,2:T(8,128)(2,1)S(1)} %copy.38, bf16[1,2048,2,128]{3,1,0,2:T(8,128)(2,1)S(1)} %copy.37, bf16[2,128,2048]{2,1,0:T(8,128)(2,1)} %all-gather.6.cloned.1.call-done), kind=kOutput, calls=%fused_computation.6 | convolution fusion | flops 4296015872 | bytes 36700160 | tf_op jit(solution)/shard_map/klbc,kcd->lbd/dot_general | solution.py:180
  549.1 171.7 %reduce-scatter.2.cloned.1.call-done = f32[256,2,2048]{2,0,1:T(8,128)} async-done(((f32[2048,2,2048]{2,0,1:T(8,128)}), f32[256,2,2048]{2,0,1:T(8,128)}) %reduce-scatter.2.cloned.1.call-update) | async-done | bytes 4194320 | tf_op jit(solution)/shard_map/reduce_scatter | solution.py:179
  723.3 3.5 copy.43
  (746 shorter events, 182.8 us)
Async XLA Ops:
  7.4 155.2 %copy-start = (bf16[2,1,128,128]{3,2,1,0:T(8,128)(2,1)S(1)}, bf16[2,1,128,128]{3,2,1,0:T(8,128)(2,1)}, u32[]{:S(2)}) copy-start(bf16[2,1,128,128]{3,2,1,0:T(8,128)(2,1)} %param.30) | copy-start | bytes 196612
  7.4 68.2 %all-gather.8.cloned.1.call-start = ((), (), s32[]{:S(2)}) async-start(), calls=%async_computation.6 | async-start | bytes 9437184 | tf_op jit(solution)/shard_map/all_gather | solution.py:30
  18.3 105.0 %all-gather.10.cloned.1.call-start = ((), (), s32[]{:S(2)}) async-start(), calls=%async_computation.7 | async-start | bytes 9437184 | tf_op jit(solution)/shard_map/all_gather | solution.py:30
  21.1 8.6 %copy-start.113 = (bf16[4,128]{1,0:T(4,128)(2,1)S(1)}, bf16[4,128]{1,0:T(4,128)(2,1)}, u32[]{:S(2)}) copy-start(bf16[4,128]{1,0:T(4,128)(2,1)} %param.27) | copy-start | bytes 3076
  21.1 8.6 %copy-start.114 = (bf16[3,128]{1,0:T(4,128)(2,1)S(1)}, bf16[3,128]{1,0:T(4,128)(2,1)}, u32[]{:S(2)}) copy-start(bf16[3,128]{1,0:T(4,128)(2,1)} %param.28) | copy-start | bytes 2308
  21.1 8.6 %copy-start.45 = (bf16[2,1024,16]{1,2,0:T(8,128)(2,1)S(1)}, bf16[2,1024,16]{1,2,0:T(8,128)(2,1)}, u32[]{:S(2)}) copy-start(bf16[2,1024,16]{1,2,0:T(8,128)(2,1)} %param.35) | copy-start | bytes 196612
  21.1 10.2 %copy-start.115 = (f32[2,128]{1,0:T(2,128)S(1)}, f32[2,128]{1,0:T(2,128)}, u32[]{:S(2)}) copy-start(f32[2,128]{1,0:T(2,128)} %param.31) | copy-start | bytes 3076
  21.1 47.6 %all-to-all-start = ((bf16[16,128,640]{2,1,0:T(8,128)(2,1)}), bf16[16,128,640]{2,1,0:T(8,128)(2,1)S(1)}, u32[]{:S(2)}, u32[]{:S(2)}) async-start(bf16[16,128,640]{2,1,0:T(8,128)(2,1)} %broadcast_in_dim.26), calls=%async_computation | async-start | bytes 5242880 | tf_op jit(solution)/shard_map/all_to_all | solution.py:12
  68.7 405.1 %all-to-all-start.2 = ((bf16[8,2,2048]{2,1,0:T(2,128)(2,1)}), bf16[8,2,2048]{2,1,0:T(2,128)(2,1)S(1)}, u32[]{:S(2)}, u32[]{:S(2)}) async-start(bf16[8,2,2048]{2,1,0:T(2,128)(2,1)} %reshape.170), calls=%async_computation.2 | async-start | bytes 131072 | tf_op jit(solution)/shard_map/all_to_all | solution.py:176
  141.0 7.5 %collective-permute-start = (bf16[2,512]{1,0:T(2,128)(2,1)S(1)}, bf16[2,512]{1,0:T(2,128)(2,1)S(1)}, u32[]{:S(2)}, u32[]{:S(2)}) collective-permute-start(bf16[2,512]{1,0:T(2,128)(2,1)S(1)} %slice.1072), channel_id=1, source_target_pairs={{0,8},{8,16},{16,24},{24,32},{32,40},{40,48},{48,56},{56,64},{64,7... | collective-permute-start | bytes 6152 | tf_op jit(solution)/shard_map/ppermute | solution.py:38
  144.1 4.3 collective-permute-start.1
  304.9 8.9 %copy-start.17 = (f32[1024,256]{1,0:T(8,128)S(1)}, f32[1024,256]{1,0:T(8,128)}, u32[]{:S(2)}) copy-start(f32[1024,256]{1,0:T(8,128)} %slice.943) | copy-start | bytes 3145732
  313.8 14.0 %copy-start.18 = (f32[1024,256]{1,0:T(8,128)S(1)}, f32[1024,256]{1,0:T(8,128)}, u32[]{:S(2)}) copy-start(f32[1024,256]{1,0:T(8,128)} %slice.1000) | copy-start | bytes 3145732
  360.4 17.9 %copy-start.16 = (f32[1023,256]{1,0:T(8,128)S(1)}, f32[1023,256]{1,0:T(8,128)}, u32[]{:S(2)}) copy-start(f32[1023,256]{1,0:T(8,128)} %slice.1050) | copy-start | bytes 3142660
  372.8 11.0 %copy-start.108 = (f32[1,256]{1,0:T(1,128)S(1)}, f32[1,256]{1,0:T(1,128)}, u32[]{:S(2)}) copy-start(f32[1,256]{1,0:T(1,128)} %get-tuple-element.248) | copy-start | bytes 3076
  372.8 11.0 %copy-start.109 = (f32[1,256]{1,0:T(1,128)S(1)}, f32[1,256]{1,0:T(1,128)}, u32[]{:S(2)}) copy-start(f32[1,256]{1,0:T(1,128)} %get-tuple-element.249) | copy-start | bytes 3076
  372.8 11.1 %copy-start.68 = (f32[2,256]{1,0:T(2,128)S(1)}, f32[2,256]{1,0:T(2,128)}, u32[]{:S(2)}) copy-start(f32[2,256]{1,0:T(2,128)} %pad_add_fusion.3) | copy-start | bytes 6148
  372.8 11.1 %copy-start.67 = (f32[2,256]{1,0:T(2,128)S(1)}, f32[2,256]{1,0:T(2,128)}, u32[]{:S(2)}) copy-start(f32[2,256]{1,0:T(2,128)} %pad_add_fusion.2) | copy-start | bytes 6148
  372.8 11.1 %copy-start.106 = (f32[1,256]{1,0:T(1,128)S(1)}, f32[1,256]{1,0:T(1,128)}, u32[]{:S(2)}) copy-start(f32[1,256]{1,0:T(1,128)} %get-tuple-element.250) | copy-start | bytes 3076
  372.8 11.1 %copy-start.107 = (f32[1,256]{1,0:T(1,128)S(1)}, f32[1,256]{1,0:T(1,128)}, u32[]{:S(2)}) copy-start(f32[1,256]{1,0:T(1,128)} %get-tuple-element.251) | copy-start | bytes 3076
  372.8 11.2 %copy-start.61 = (f32[3,256]{1,0:T(4,128)S(1)}, f32[3,256]{1,0:T(4,128)}, u32[]{:S(2)}) copy-start(f32[3,256]{1,0:T(4,128)} %slice.897) | copy-start | bytes 9220
  372.8 11.2 %copy-start.62 = (f32[3,256]{1,0:T(4,128)S(1)}, f32[3,256]{1,0:T(4,128)}, u32[]{:S(2)}) copy-start(f32[3,256]{1,0:T(4,128)} %slice.880) | copy-start | bytes 9220
  372.9 11.2 %copy-start.100 = (f32[1,256]{1,0:T(1,128)S(1)}, f32[1,256]{1,0:T(1,128)}, u32[]{:S(2)}) copy-start(f32[1,256]{1,0:T(1,128)} %slice.1088) | copy-start | bytes 3076
  372.9 11.2 %copy-start.101 = (f32[1,256]{1,0:T(1,128)S(1)}, f32[1,256]{1,0:T(1,128)}, u32[]{:S(2)}) copy-start(f32[1,256]{1,0:T(1,128)} %slice.1123) | copy-start | bytes 3076
  372.9 11.3 %copy-start.57 = (f32[7,256]{1,0:T(8,128)S(1)}, f32[7,256]{1,0:T(8,128)}, u32[]{:S(2)}) copy-start(f32[7,256]{1,0:T(8,128)} %slice.899) | copy-start | bytes 21508
  372.9 11.3 %copy-start.58 = (f32[7,256]{1,0:T(8,128)S(1)}, f32[7,256]{1,0:T(8,128)}, u32[]{:S(2)}) copy-start(f32[7,256]{1,0:T(8,128)} %slice.874) | copy-start | bytes 21508
  372.9 11.3 %copy-start.98 = (f32[1,256]{1,0:T(1,128)S(1)}, f32[1,256]{1,0:T(1,128)}, u32[]{:S(2)}) copy-start(f32[1,256]{1,0:T(1,128)} %slice.1087) | copy-start | bytes 3076
  372.9 11.3 %copy-start.99 = (f32[1,256]{1,0:T(1,128)S(1)}, f32[1,256]{1,0:T(1,128)}, u32[]{:S(2)}) copy-start(f32[1,256]{1,0:T(1,128)} %slice.1122) | copy-start | bytes 3076
  372.9 11.4 %copy-start.47 = (f32[15,256]{1,0:T(8,128)S(1)}, f32[15,256]{1,0:T(8,128)}, u32[]{:S(2)}) copy-start(f32[15,256]{1,0:T(8,128)} %slice.901) | copy-start | bytes 46084
  372.9 11.4 %copy-start.48 = (f32[15,256]{1,0:T(8,128)S(1)}, f32[15,256]{1,0:T(8,128)}, u32[]{:S(2)}) copy-start(f32[15,256]{1,0:T(8,128)} %slice.868) | copy-start | bytes 46084
  372.9 11.4 %copy-start.94 = (f32[1,256]{1,0:T(1,128)S(1)}, f32[1,256]{1,0:T(1,128)}, u32[]{:S(2)}) copy-start(f32[1,256]{1,0:T(1,128)} %slice.1086) | copy-start | bytes 3076
  372.9 11.4 %copy-start.95 = (f32[1,256]{1,0:T(1,128)S(1)}, f32[1,256]{1,0:T(1,128)}, u32[]{:S(2)}) copy-start(f32[1,256]{1,0:T(1,128)} %slice.1121) | copy-start | bytes 3076
  407.0 20.0 %copy-start.5 = (f32[2048,256]{1,0:T(8,128)}, f32[2048,256]{1,0:T(8,128)S(1)}, u32[]{:S(2)}) copy-start(f32[2048,256]{1,0:T(8,128)S(1)} %pad.310) | copy-start | bytes 6291460
  412.0 10.2 %copy-start.14 = (f32[1024,256]{1,0:T(8,128)S(1)}, f32[1024,256]{1,0:T(8,128)}, u32[]{:S(2)}) copy-start(f32[1024,256]{1,0:T(8,128)} %add.594) | copy-start | bytes 3145732
  420.8 7.8 %copy-start.55 = (f32[7,256]{1,0:T(8,128)S(1)}, f32[7,256]{1,0:T(8,128)}, u32[]{:S(2)}) copy-start(f32[7,256]{1,0:T(8,128)} %slice.1036) | copy-start | bytes 21508
  420.8 7.8 %copy-start.92 = (f32[1,256]{1,0:T(1,128)S(1)}, f32[1,256]{1,0:T(1,128)}, u32[]{:S(2)}) copy-start(f32[1,256]{1,0:T(1,128)} %slice.1194) | copy-start | bytes 3076
  420.8 7.8 %copy-start.93 = (f32[1,256]{1,0:T(1,128)S(1)}, f32[1,256]{1,0:T(1,128)}, u32[]{:S(2)}) copy-start(f32[1,256]{1,0:T(1,128)} %slice.1158) | copy-start | bytes 3076
  420.8 7.9 %copy-start.46 = (f32[15,256]{1,0:T(8,128)S(1)}, f32[15,256]{1,0:T(8,128)}, u32[]{:S(2)}) copy-start(f32[15,256]{1,0:T(8,128)} %slice.981) | copy-start | bytes 46084
  422.2 8.1 %copy-start.41 = (f32[31,256]{1,0:T(8,128)S(1)}, f32[31,256]{1,0:T(8,128)}, u32[]{:S(2)}) copy-start(f32[31,256]{1,0:T(8,128)} %slice.1040) | copy-start | bytes 95236
  422.2 8.1 %copy-start.42 = (f32[31,256]{1,0:T(8,128)S(1)}, f32[31,256]{1,0:T(8,128)}, u32[]{:S(2)}) copy-start(f32[31,256]{1,0:T(8,128)} %slice.983) | copy-start | bytes 95236
  422.2 9.6 %copy-start.37 = (f32[63,256]{1,0:T(8,128)S(1)}, f32[63,256]{1,0:T(8,128)}, u32[]{:S(2)}) copy-start(f32[63,256]{1,0:T(8,128)} %slice.1042) | copy-start | bytes 193540
  422.2 9.6 %copy-start.38 = (f32[63,256]{1,0:T(8,128)S(1)}, f32[63,256]{1,0:T(8,128)}, u32[]{:S(2)}) copy-start(f32[63,256]{1,0:T(8,128)} %slice.985) | copy-start | bytes 193540
  458.9 9.3 %copy-start.15 = (f32[1024,256]{1,0:T(8,128)S(1)}, f32[1024,256]{1,0:T(8,128)}, u32[]{:S(2)}) copy-start(f32[1024,256]{1,0:T(8,128)} %add.607) | copy-start | bytes 3145732
  467.5 15.3 %copy-start.112 = (f32[2,2,128]{2,1,0:T(2,128)S(1)}, f32[2,2,128]{2,1,0:T(2,128)}, u32[]{:S(2)}) copy-start(f32[2,2,128]{2,1,0:T(2,128)} %param.34) | copy-start | bytes 6148
  474.5 48.5 %all-to-all-start.1 = ((f32[16,1,4,256]{3,2,1,0:T(4,128)}), f32[16,1,4,256]{3,2,1,0:T(4,128)S(1)}, u32[]{:S(2)}, u32[]{:S(2)}) async-start(f32[16,1,4,256]{3,2,1,0:T(4,128)} %broadcast_in_dim.27), calls=%async_computation.1 | async-start | bytes 131072 | tf_op jit(solution)/shard_map/all_to_all | solution.py:12
  482.7 52.6 %all-gather.6.cloned.1.call-start = ((), (), s32[]{:S(2)}) async-start(), calls=%async_computation.4 | async-start | bytes 1114112 | tf_op jit(solution)/shard_map/all_gather | solution.py:177
  484.3 236.5 %reduce-scatter.2.cloned.1.call-start = ((), (), s32[]{:S(2)}) async-start(), calls=%async_computation.5 | async-start | bytes 37748736 | tf_op jit(solution)/shard_map/reduce_scatter | solution.py:179
  506.3 20.1 %copy-start.6 = (f32[2048,256]{1,0:T(8,128)S(1)}, f32[2048,256]{1,0:T(8,128)}, u32[]{:S(2)}) copy-start(f32[2048,256]{1,0:T(8,128)} %copy-done.5) | copy-start | bytes 6291460
  (77 other events, 260.2 us)
Sparse Core Ops, SparseCore 0:
  18.5 53.2 all-gather.7
  73.5 49.8 all-gather.9
  549.2 171.5 reduce-scatter.1
Sparse Core Ops, SparseCore 1:
  485.3 43.2 all-gather.5
where the time goes:
time: 745 us; the launch traced here: 734 us
  local copies, waits for them, and re-layouts  328 us (44%)
  waiting for transfers between devices  249 us (33%)
  other arithmetic  75.3 us (10%)
  matrix products  34.8 us (5%)
  starting transfers between devices  28.3 us (4%)
  between operations  17.7 us (2%)
    slice x158, local copies, waits for them, and re-layouts, body(): lax.associative_scan(combine, (decay, drive), axis=0, reverse=scan_direct...  181 us
    reduce_scatter x1, waiting for transfers between devices, body(): lax.psum_scatter(jnp.einsum('klbc,kcd->lbd', part_rows, own_weight, prefe...  172 us
    pad x80, local copies, waits for them, and re-layouts, body(): lax.associative_scan(combine, (decay, drive), axis=0, reverse=scan_direct...  60.5 us
    all_gather x2, waiting for transfers between devices, on_gathered_pieces(): parts = [lax.all_gather(share, axis) for share in pieces]  37.9 us
    all_to_all x2, waiting for transfers between devices, sent_to_all(): return lax.all_to_all(copies, axis, split_axis=0, concat_axis=0, tiled=True)  37.4 us
    rev x2, local copies, waits for them, and re-layouts, body(): lax.associative_scan(combine, (decay, drive), axis=0, reverse=scan_direct...  27.1 us
    add x46, other arithmetic, body(): lax.associative_scan(combine, (decay, drive), axis=0, reverse=scan_direct...  22.6 us
    dot_general x2, matrix products, project(): jnp.dot(piece, in_weights, preferred_element_type=jnp.float32)  19.8 us
  transfers between devices with their start and end apart: 9, of which 4 were waited for; matrix products, arithmetic and copies ran while one was open for 54% of the time, Pallas kernels for 0%

commit v1 on v0

v1 whole, which is shorter than its diff:
```python
import jax
import jax.numpy as jnp
from jax import lax
from jax.experimental import pallas as pl
from jax.experimental.pallas import tpu as pltpu
from jax.sharding import PartitionSpec as P

MESH = pl.DeviceIdType.MESH
f32, bf16 = jnp.float32, jnp.bfloat16

EPS = 1e-06
RING = 4
OWN = 512
STEPS = 64
WIDE = 2048
LANES = 128
POOL = 32

SRC, GATES, CGATE, CIN, COUT, EXIT, W_END = 0, 128, 160, 288, 416, 544, 672
OUT_ROWS = 256

PIECES = (
    ("w", ((0, 64), (64, 112), (112, 160))),
    ("w", ((160, 240), (240, 320), (320, 416))),
    ("w", ((416, 496), (496, 592), (592, 672))),
    ("o", ((0, 80), (80, 160), (160, 256))),
)
ORDERS = (("y", "x", "z"), ("x", "z", "y"), ("z", "y", "x"))
NEAR = (0, -1, 1, 2)
FORWARD = {1: (0, -1), -1: (1, 2)}


def turn_of(piece):
    return 1 if piece % 2 == 0 else -1


def group_of(m):
    piece, colour, phase, kind, way, r = m
    if kind == "pass":
        return (piece, colour, 3, r, 1)
    if phase == 0:
        return (piece, colour, 0, 2 if kind == "fwd" else (0 if way == 1 else 1), 1)
    first = 3 + 7 * (phase - 1)
    if kind == "fwd":
        return (piece, colour, phase, first + 6, 4)
    alone = FORWARD[way]
    place = alone.index(r) if r in alone else 2
    return (piece, colour, phase, first + place + (0 if way == 1 else 3), 1 if r in alone else 2)


def messages(piece, colour):
    found = {}
    up = turn_of(piece)

    def own(phase, way, r):
        return (piece, colour, phase, "own", way, r)

    def fwd(phase, way, r):
        return (piece, colour, phase, "fwd", way, r)

    def here(*given):
        return tuple(dict.fromkeys(group_of(m) for m in given))

    ready = {-1: here(own(0, 1, 0)), 1: here(own(0, -1, 0)), 2: here(fwd(0, up, 0)), 0: ()}
    first = here(own(0, 1, 0), own(0, -1, 0), fwd(0, up, 0))
    for way in (1, -1):
        found[own(0, way, 0)] = ()
    found[fwd(0, up, 0)] = here(own(0, up, 0))
    for phase in (1, 2):
        for r in NEAR:
            for way in (1, -1):
                found[own(phase, way, r)] = ready[r]
        for way in (1, -1):
            for r in FORWARD[way]:
                found[fwd(phase, way, r)] = here(own(phase, way, r))
        ready = {
            0: first,
            -1: here(*(own(phase, 1, r) for r in NEAR)),
            1: here(*(own(phase, -1, r) for r in NEAR)),
            2: here(fwd(phase, 1, 0)),
        }
    if piece == 3:
        before = here(*(m for m in found if m[2] < 2))
        for slot, r in enumerate((0, -1, 1, 2)):
            found[(piece, colour, 3, "pass", 0, slot)] = before if r == 0 else ready[r]
    return found


def size(m):
    first, last = PIECES[m[0]][1][m[1]]
    return (last - first) * 0.25 * (1, 1, 4, 16)[m[2]]


RATE, HOP = 44.0, 2.2
SIDE_RATE, SIDE_HOP = 450.0, 1.4

STAGES = (
    ("norm_own", 4, 1.5, ()),
    ("norm_other", 4, 1.5, ("rows",)),
    ("norm_edges", 1, 0.3, ("edges",)),
    ("source", 4, 0.8, ("norm_own", "norm_other", "norm_edges", 0)),
    ("source_edges", 1, 0.6, ("source",)),
    ("gates", 4, 1.95, ("source_edges", "small")),
    ("totals", 1, 1.3, ("gates",)),
    ("hear0", 1, 0.4, ("told0",)),
    ("hear1", 1, 0.4, ("told1",)),
    ("hear2", 1, 0.5, ("told2",)),
    ("shake", 4, 1.4, ("norm_own", "norm_other", "norm_edges", 1)),
    ("shake_edges", 1, 0.8, ("shake",)),
    ("exit_gate", 4, 0.78, (2, "norm_other")),
    ("conv", 4, 0.75, (2, "shake_edges")),
    ("states", 1, 1.5, ("hear2", "exit_gate")),
    ("result", 8, 0.85, (3, "swapped0", "swapped1")),
)
BACKLOG = 1.0


def PRIORITY(m):
    return (m[0], m[2])


def plan():
    deps = {}
    for piece in range(4):
        for colour in range(3):
            deps.update(messages(piece, colour))
    groups = {}
    for m in deps:
        groups.setdefault(group_of(m), []).append(m)
    clock, link, coming, arrive, sent, got = 0.0, {}, {}, {}, set(), set()
    times = {"rows": 6.0, "edges": 4.0, "small": 6.0}
    order, done, progress = [], set(), {}

    def send_ready():
        ready = [m for m in deps if m not in sent and all(d in got for d in deps[m])]
        for m in sorted(ready, key=PRIORITY):
            side = m[3] == "pass"
            wire = "side" if side else (ORDERS[m[1]][m[2]], m[4])
            if link.get(wire, 0.0) - clock > BACKLOG:
                continue
            link[wire] = max(clock, link.get(wire, 0.0)) + size(m) / (SIDE_RATE if side else RATE)
            arrive[m] = link[wire] + (SIDE_HOP if side else HOP)
            sent.add(m)
            order.append(("send", m))
            g = group_of(m)
            if all(n in sent for n in groups[g]):
                coming[g] = max(arrive[n] for n in groups[g])

    def met(need):
        if isinstance(need, int):
            return all(g in got for g in groups if g[0] == need)
        return need in done or times.get(need, 1e9) <= clock

    current = None
    send_ready()
    while len(done) < len(STAGES):
        here = sorted((m for m in coming if m not in got and coming[m] <= clock), key=lambda m: (m[0], coming[m]))
        if here:
            m = here[0]
            got.add(m)
            order.append(("wait", m))
            clock += 0.03
            send_ready()
            continue
        send_ready()
        if current is None:
            for n, stage in enumerate(STAGES):
                if stage[0] not in done and all(met(need) for need in stage[3]):
                    current = stage
                    break
        quick = next(
            (st for st in STAGES if st[0].startswith("hear") and st[0] not in done and all(met(k) for k in st[3])), None
        )
        if quick is not None:
            order.append(("unit", quick[0], 0))
            clock += quick[2]
            done.add(quick[0])
            level = int(quick[0][4])
            if level < 2:
                times[f"told{level + 1}"] = clock + 3.5
            if current is quick:
                current = None
            continue
        if current is not None:
            name, units, cost, _ = current
            i = progress.get(name, 0)
            order.append(("unit", name, i))
            clock += cost
            progress[name] = i + 1
            if i + 1 == units:
                done.add(name)
                current = None
                if name == "totals":
                    times["told0"] = clock + 3.5
                if name == "conv":
                    times["swapped1"] = clock + 3.0
                if name == "states":
                    times["swapped0"] = clock + 3.0
            continue
        if any(m not in sent and all(d in got for d in deps[m]) for m in deps):
            clock += 0.25
            continue
        later = [t for m, t in coming.items() if m not in got] + [t for t in times.values() if t > clock]
        clock = min(t for t in later if t > clock)
    return order, clock


def wrap(i):
    return lax.rem(i + RING, RING)


def rows_of(shape):
    return lax.broadcasted_iota(jnp.int32, shape, 0)


def turn(v, by):
    return pltpu.roll(v, by, 0)


def spread(v, first):
    row = rows_of(v.shape)
    v = jnp.where((row >= first) & (row < first + 2), v, 0.0)
    v = v + turn(v, 2)
    return v + turn(v, 4)


def kernel(
    x_in, gain_in, src_in, exit_in, cout_in, cgate_in, cin_in, taps_in, ctaps_in, fade_in, entry_in, speed_in,
    tempo_in, jump_in, edge_in, out_w, out,
    XR, XE, X, G, Wo, GN, TB, CB, SB, BB, PM, SM, MJ, Rp, Sp, Hh, A, U, GL, ACT, ACTS, SEG, PRE, XS,
    lsem, wsem, pool, grecv, frecv, xrecv, hrecv, srecv, erecv, arecv,
):
    sp, tp = lax.axis_index("sp"), lax.axis_index("tp")
    me = {"z": sp // 4, "x": lax.rem(sp, 4), "y": tp // 2}
    c = lax.rem(tp, 2)
    z, x, y = me["z"], me["x"], me["y"]
    q = sp * 4 + y

    def device(at, core):
        return {"sp": at["z"] * 4 + at["x"], "tp": at["y"] * 2 + core}

    def along(d, by):
        return {**me, d: wrap(me[d] + by)}

    sibling = device(me, 1 - c)
    ahead = lax.rem(q + 1, 64)
    behind = lax.rem(q + 63, 64)

    def chip(number, core):
        return {"sp": number // 4, "tp": lax.rem(number, 4) * 2 + core}

    barrier = pltpu.get_barrier_semaphore()

    def hello(to):
        pl.semaphore_signal(barrier, inc=1, device_id=to, device_id_type=MESH)

    hello(sibling)
    for d in ("z", "x", "y"):
        for by in (1, 2, 3):
            hello(device(along(d, by), c))
    hello(chip(behind, 1))
    hello(chip(ahead, 0))

    def own_rows(first, count):
        return G.at[z, x, y, pl.ds(first, count)]

    sp16 = pl.ds(pl.multiple_of(sp * 16, 16), 16)
    pairs = [
        (src_in, own_rows(SRC, 128)),
        (fade_in.at[sp16], own_rows(GATES, 16)),
        (entry_in.at[sp16], own_rows(GATES + 16, 16)),
        (cgate_in, own_rows(CGATE, 128)),
        (cin_in, own_rows(CIN, 128)),
        (cout_in, own_rows(COUT, 128)),
        (exit_in, own_rows(EXIT, 128)),
        (gain_in, GN),
        (taps_in, TB),
        (ctaps_in, CB),
        (speed_in, SB),
        (edge_in, BB),
        (tempo_in, PM.at[0]),
        (jump_in, PM.at[1]),
    ]
    pairs += [(x_in.at[pl.ds(seg * STEPS, STEPS)], XR.at[c, :, seg]) for seg in range(4)]
    local = [pltpu.make_async_copy(a, b, lsem.at[n]) for n, (a, b) in enumerate(pairs)]
    out_local = [
        pltpu.make_async_copy(
            out_w.at[n // 8, :, pl.ds((n % 8) * LANES, LANES)], Wo.at[z, x, y, c, pl.ds(n * 16, 16)], wsem.at[n]
        )
        for n in range(16)
    ]
    for copy in local + out_local:
        copy.start()
    pl.semaphore_wait(barrier, 12)

    def remote(src, dst, send, recv, to):
        return pltpu.make_async_remote_copy(
            src_ref=src, dst_ref=dst, send_sem=pool.at[0] if send is None else send, recv_sem=recv, device_id=to, device_id_type=MESH
        )

    sends = []

    def go(make, *given):
        n = len(sends)
        if n >= POOL:
            finish(n - POOL)
        make(*given, send=pool.at[n % POOL]).start()
        sends.append((make, given))

    def finish(n):
        make, given = sends[n]
        make(*given, send=pool.at[n % POOL]).wait_send()

    def rows_copy(seg, send=None):
        return remote(
            x_in.at[pl.ds(seg * STEPS, STEPS)], XR.at[c, :, seg], send, xrecv.at[seg], sibling
        )

    target = jnp.where(c == 1, ahead, behind)

    def edge_copy(core, slot, send=None):
        return remote(
            x_in.at[pl.ds(c * 254, 2)], XE.at[pl.ds((1 - c) * 2, 2)], send, hrecv.at[slot], chip(target, core)
        )

    for seg in range(4):
        go(rows_copy, seg)
    for core in range(2):
        go(edge_copy, core, 1 - c)

    def region(piece, colour, phase, i, r, count=1):
        kind, parts = PIECES[piece]
        first, last = parts[colour]
        a, b, d = ORDERS[colour]
        where = dict(me)
        if phase == 0:
            where[a] = i
        elif phase == 1:
            where[a], where[b] = wrap(me[a] + r), i
        else:
            where[a], where[b], where[d] = slice(None), wrap(me[b] + r), i
            if phase == 3:
                where[b] = slice(None)
        if count > 1:
            where[(a, b)[phase - 1]] = pl.ds(0, count)
        rows = pl.ds(first, last - first)
        if kind == "w":
            return G.at[where["z"], where["x"], where["y"], rows]
        return Wo.at[where["z"], where["x"], where["y"], c, rows]

    def message(m, send=None):
        piece, colour, phase, kind, way, r = m
        if kind == "pass":
            d = ORDERS[colour][2]
            ref = region(piece, colour, 3, wrap(me[d] + (0, -1, 1, 2)[r]), 0)
            return remote(ref, ref, send, frecv.at[colour, r], sibling)
        d = ORDERS[colour][phase]
        block = me[d] if kind == "own" else wrap(me[d] - way)
        ref = region(piece, colour, phase, block, r)
        return remote(ref, ref, send, grecv.at[(piece * 3 + colour) * 17 + group_of(m)[3]], device(along(d, way), c))

    def group_here(g):
        piece, colour, phase, place, count = g
        ref = region(piece, colour, phase, 0, 0, count)
        remote(ref, ref, None, grecv.at[(piece * 3 + colour) * 17 + place], sibling).wait_recv()

    for copy in local[7:14]:
        copy.wait()
    for row in range(4):
        SM[y, row : row + 1, :] = TB[row : row + 1, :].astype(f32)
    for row in range(3):
        SM[y, 4 + row : 5 + row, :] = CB[row : row + 1, :].astype(f32)
    for row in range(2):
        SM[y, 7 + row : 8 + row, :] = SB[row : row + 1, :]
        for b in range(2):
            SM[y, 9 + 2 * row + b : 10 + 2 * row + b, :] = BB[row, b : b + 1, :]
    SM[y, 13:16, :] = jnp.zeros((3, LANES), f32)

    def small_copy(by, send=None):
        return remote(SM.at[y], SM.at[y], send, srecv.at[by - 1], device(along("y", by), c))

    def positions():
        seg = rows_of((8, LANES)) // 2
        for n in range(2):
            for rc in range(2):
                lines = [
                    jnp.broadcast_to(PM[n, pl.ds(4 * y + rc * 2 + k, 1), :], (8, LANES)) for k in range(2)
                ]
                v = jnp.where(
                    seg == 0,
                    lines[0],
                    jnp.where(
                        seg == 1, pltpu.roll(lines[0], 64, 1), jnp.where(seg == 2, lines[1], pltpu.roll(lines[1], 64, 1))
                    ),
                )
                for j in range(STEPS):
                    MJ[n, rc * OWN + j * 8 : rc * OWN + j * 8 + 8, :] = jnp.broadcast_to(v[:, j : j + 1], (8, LANES))

    def scaled(parts, alive=None):
        total = parts[0] * parts[0]
        for v in parts[1:]:
            total = total + v * v
        r = lax.rsqrt(jnp.sum(total, axis=1, keepdims=True) * (1.0 / WIDE) + EPS)
        if alive is not None:
            r = r * alive
        r = jnp.broadcast_to(r, parts[0].shape)
        return [(v * r) * GN[n : n + 1, :].astype(f32) for n, v in enumerate(parts)]

    def norm_unit(rc, i):
        def one(k, _):
            j = i * 16 + k * 2
            parts = [
                XR[rc, pl.ds(j, 2), :, :, n * LANES : (n + 1) * LANES].astype(f32).reshape(16, LANES) for n in range(16)
            ]
            rows = pl.ds(pl.multiple_of(rc * OWN + j * 8, 16), 16)
            for n, v in enumerate(scaled(parts)):
                X[rows, n * LANES : (n + 1) * LANES] = v.astype(bf16)
            return 0

        lax.fori_loop(0, 8, one, 0)

    def norm_edges():
        row = rows_of((8, 1))
        alive = jnp.where(row < 4, jnp.where(q > 0, 1.0, 0.0), jnp.where(q < 63, 1.0, 0.0))
        parts = [XE[:, :, n * LANES : (n + 1) * LANES].astype(f32).reshape(8, LANES) for n in range(16)]
        for n, v in enumerate(scaled(parts, alive)):
            lane = slice(n * LANES, (n + 1) * LANES)
            X[2 * OWN : 2 * OWN + 16, lane] = jnp.concatenate([turn(v, 6), turn(v, 4)], axis=0).astype(bf16)
            X[2 * OWN + 16 : 2 * OWN + 32, lane] = jnp.concatenate([turn(v, 4), turn(v, 4)], axis=0).astype(bf16)

    def weight(row, yp):
        parts = [G[:, :, 2 * yp + h, pl.ds(row, LANES), :].reshape(WIDE, LANES) for h in range(2)]
        return jnp.concatenate(parts, axis=1)

    def project(rows, w):
        return jnp.dot(X[rows, :], w, preferred_element_type=f32)

    def block(work, i):
        yp, rc = i // 2, lax.rem(i, 2)
        work(yp, rc, pl.ds(pl.multiple_of(rc * OWN, OWN), OWN))

    main = pl.ds(16, OWN)
    edges = pl.ds(2 * OWN, 32)

    def pads(Rp):
        for yp in range(2):
            row = rows_of((8, 256))
            for rc in range(2):
                for j in range(2):
                    own = Rp[yp, rc, pl.ds(16 + (STEPS - 2 + j) * 8, 8), :]
                    prior = Hh[yp, pl.ds(8 * j, 8), :] if rc == 0 else Rp[yp, 0, pl.ds(16 + (STEPS - 2 + j) * 8, 8), :]
                    Rp[yp, rc, pl.ds(8 * j, 8), :] = jnp.where(row < 2, turn(prior, 2), turn(own, 2))
                own = Rp[yp, rc, pl.ds(16, 8), :]
                later = Rp[yp, 1, pl.ds(16, 8), :] if rc == 0 else Hh[yp, pl.ds(16, 8), :]
                Rp[yp, rc, pl.ds(16 + OWN, 8), :] = jnp.where(row >= 6, turn(later, 6), turn(own, 6))

    def source(i):
        def work(yp, rc, rows):
            Rp[yp, rc, main, :] = project(rows, weight(SRC, yp))

        block(work, i)

    def source_edges():
        for yp in range(2):
            Hh[yp] = project(edges, weight(SRC, yp))
        pads(Rp)

    def taps(yp, row):
        return jnp.concatenate([SM[2 * yp + h, pl.ds(row, 1), :] for h in range(2)], axis=1)

    GB = 128

    def gates(i):
        def one(k, _):
            gate_rows(i // 2, lax.rem(i, 2), k)
            return 0

        lax.fori_loop(0, 4, one, 0)

    def gate_rows(yp, rc, blk):
        base = pl.multiple_of(blk * GB, GB)
        rc_rows = jnp.zeros((GB, 256), f32)
        for k in range(4):
            rc_rows = rc_rows + taps(yp, k) * Rp[yp, rc, pl.ds(base + 8 * k, GB), :]
        narrow = rc_rows.astype(bf16)
        wide = narrow.astype(f32)
        at = pl.ds(pl.multiple_of(rc * OWN + blk * GB, GB), GB)
        tempo, jump = MJ[0, at, :], MJ[1, at, :]
        for h in range(2):
            lane = slice(h * LANES, (h + 1) * LANES)
            yy = 2 * yp + h
            maps = [
                    G[pl.ds(2 * d, 2), :, yy, pl.ds(GATES + 16 * kind, 16), :].reshape(LANES, LANES)
                    for kind in range(2)
                    for d in range(2)
                ]
            for d in range(2):
                pre = jnp.dot(
                    narrow[:, lane], jnp.concatenate([maps[d], maps[2 + d]], axis=1), preferred_element_type=f32
                )
                speed = SM[yy, pl.ds(7 + d, 1), :] * -4.0
                la = (1.0 + jnp.tanh(0.5 * pre[:, :LANES])) * (speed * tempo) + jump
                decay = jnp.exp(la)
                t = 2.0 * la
                near = -t * (1.0 + t * (0.5 + t * (1.0 / 6.0 + t * (1.0 / 24.0 + t * (1.0 / 120.0)))))
                rest = jnp.where(t > -0.1, near, 1.0 - decay * decay)
                opening = 0.5 + 0.5 * jnp.tanh(0.5 * pre[:, LANES:])
                A[d, yp, rc, pl.ds(base, GB), lane] = decay
                U[d, yp, rc, pl.ds(base, GB), lane] = jnp.sqrt(rest) * opening * wide[:, lane]

    PAIRS = [(yp, rc) for yp in range(2) for rc in range(2)]

    def tile(ref, d, yp, rc, j):
        return ref[d, yp, rc, pl.ds(pl.multiple_of(j * 8, 8), 8), :]

    def totals():
        def one(i, state):
            new = []
            for d in range(2):
                j = i if d == 0 else STEPS - 1 - i
                for n, (yp, rc) in enumerate(PAIRS):
                    sa, sb = state[d * 4 + n]
                    a = tile(A, d, yp, rc, j)
                    new.append((sa * a, sb * a + tile(U, d, yp, rc, j)))
            return tuple(new)

        start = tuple((jnp.ones((8, 256), f32), jnp.zeros((8, 256), f32)) for _ in range(8))
        end = lax.fori_loop(0, STEPS, one, start)
        row = rows_of((8, 256))
        for yp in range(2):
            whole = []
            for d in range(2):
                ends = []
                for rc in range(2):
                    a, b = end[d * 4 + yp * 2 + rc]
                    for by in (2, 4):
                        shift = by if d == 0 else 8 - by
                        inside = (row >= by) if d == 0 else (row < 8 - by)
                        pa, pb = turn(a, shift), turn(b, shift)
                        b = jnp.where(inside, a * pb + b, b)
                        a = jnp.where(inside, a * pa, a)
                    SEG[d, yp, rc, 0], SEG[d, yp, rc, 1] = a, b
                    ends.append((spread(a, 6 if d == 0 else 0), spread(b, 6 if d == 0 else 0)))
                first, second = ends if d == 0 else ends[::-1]
                whole.append((first[0] * second[0], second[0] * first[1] + second[1]))
            put(0, y, yp, whole)

    def put(level, slot, yp, whole):
        row = rows_of((8, 256))
        (fa, fb), (ba, bb) = whole
        XS[level, slot, :, yp * 256 : (yp + 1) * 256] = jnp.where(
            row < 2, fa, jnp.where(row < 4, fb, jnp.where(row < 6, ba, bb))
        )

    AXES = ("y", "x", "z")

    def share(level, by, send=None):
        d = AXES[level]
        ref = XS.at[level, me[d]]
        k = level * 3 + by - 1
        return remote(ref, ref, send, erecv.at[k], device(along(d, by), c))

    def tell(level):
        for by in (1, 2, 3):
            go(share, level, by)

    def combine(early, late):
        return early[0] * late[0], late[0] * early[1] + late[1]

    def hear(level):
        for by in (1, 2, 3):
            share(level, by).wait_recv()
        m = me[AXES[level]]
        for yp in range(2):
            one = (jnp.ones((8, 256), f32), jnp.zeros((8, 256), f32))
            whole = []
            for d in range(2):
                total, prefix = one, one
                for i in range(4) if d == 0 else range(3, -1, -1):
                    v = XS[level, i, :, yp * 256 : (yp + 1) * 256]
                    item = (spread(v, 4 * d), spread(v, 4 * d + 2))
                    passed = (i < m) if d == 0 else (i > m)
                    longer = combine(prefix, item)
                    prefix = tuple(jnp.where(passed, n, o) for n, o in zip(longer, prefix))
                    total = combine(total, item)
                whole.append(total)
                PRE[level, yp, d, 0], PRE[level, yp, d, 1] = prefix
            if level < 2:
                put(level + 1, me[AXES[level + 1]], yp, whole)
        if level < 2:
            tell(level + 1)

    def entering():
        row = rows_of((8, 256))
        even = (row % 2) == 0
        for yp in range(2):
            for d in range(2):
                h = jnp.where(even, taps(yp, 9 + 2 * d), taps(yp, 10 + 2 * d))
                for level in (2, 1, 0):
                    a, b = PRE[level, yp, d, 0], PRE[level, yp, d, 1]
                    h = a * h + b
                for rc in (0, 1) if d == 0 else (1, 0):
                    a, b = SEG[d, yp, rc, 0], SEG[d, yp, rc, 1]
                    shift = 2 if d == 0 else 6
                    inside = (row >= 2) if d == 0 else (row < 6)
                    pa = jnp.where(inside, turn(a, shift), 1.0)
                    pb = jnp.where(inside, turn(b, shift), 0.0)
                    SEG[d, yp, rc, 0] = pa * h + pb
                    last = 6 if d == 0 else 0
                    h = spread(a, last) * h + spread(b, last)

    def exit_gate(i):
        def work(yp, rc, rows):
            v = project(rows, weight(EXIT, yp))
            inner = v * (0.7978845608028654 + 0.035677408136300125 * v * v)
            GL[yp, rc] = 0.5 * v * (1.0 + jnp.tanh(inner))

        block(work, i)

    def states():
        def forth(i, state):
            new = []
            for n, (yp, rc) in enumerate(PAIRS):
                h = tile(A, 0, yp, rc, i) * state[n] + tile(U, 0, yp, rc, i)
                U[0, yp, rc, pl.ds(pl.multiple_of(i * 8, 8), 8), :] = h
                new.append(h)
            return tuple(new)

        def back(i, state):
            new = []
            low = STEPS - 2 - 2 * i
            rows16 = pl.ds(pl.multiple_of(low * 8, 16), 16)
            for n, (yp, rc) in enumerate(PAIRS):
                h1 = tile(A, 1, yp, rc, low + 1) * state[n] + tile(U, 1, yp, rc, low + 1)
                h0 = tile(A, 1, yp, rc, low) * h1 + tile(U, 1, yp, rc, low)
                both = jnp.concatenate([h0, h1], axis=0) + U[0, yp, rc, rows16, :]
                done = (both * GL[yp, rc, rows16, :]).astype(bf16)
                for h in range(2):
                    ACT[rc, 0, 2 * yp + h, rows16, :] = done[:, h * LANES : (h + 1) * LANES]
                new.append(h0)
            return tuple(new)

        lax.fori_loop(0, STEPS, forth, tuple(SEG[0, yp, rc, 0] for yp, rc in PAIRS))
        lax.fori_loop(0, STEPS // 2, back, tuple(SEG[1, yp, rc, 0] for yp, rc in PAIRS))

    def shake(i):
        def work(yp, rc, rows):
            Sp[yp, rc, main, :] = project(rows, weight(CGATE, yp)) * project(rows, weight(CIN, yp))

        block(work, i)

    def shake_edges():
        for yp in range(2):
            Hh[yp] = project(edges, weight(CGATE, yp)) * project(edges, weight(CIN, yp))
        pads(Sp)

    def conv(i):
        def work(yp, rc, rows):
            v = project(rows, weight(COUT, yp))
            s = jnp.zeros((OWN, 256), f32)
            for k in range(3):
                s = s + taps(yp, 4 + k) * Sp[yp, rc, pl.ds(8 + 8 * k, OWN), :]
            done = (v * s).astype(bf16)
            for h in range(2):
                ACT[rc, 1, 2 * yp + h] = done[:, h * LANES : (h + 1) * LANES]

        block(work, i)

    def swap(m, send=None):
        return remote(ACT.at[1 - c, m], ACTS.at[m], send, arecv.at[m], sibling)

    def result(i):
        zz, xx = i // 2, lax.rem(i, 2) * 2
        left, right = [], []
        for own in range(2):
            core = c if own == 0 else 1 - c
            for m in range(2):
                for yy in range(4):
                    left.append(ACT[c, m, yy] if own == 0 else ACTS[m, yy])
                    k16 = pl.ds(pl.multiple_of((m * 8 + 2 * yy + core) * 16, 16), 16)
                    right.append(Wo[zz, pl.ds(xx, 2), :, :, k16, :].reshape(256, LANES))
        v = lax.dot_general(
            jnp.concatenate(left, axis=1), jnp.concatenate(right, axis=1),
            (((1,), (1,)), ((), ())), preferred_element_type=f32,
        )
        v = v.astype(bf16).reshape(STEPS, 4, 2, 256)
        for seg in range(4):
            out[seg * STEPS : (seg + 1) * STEPS, :, pl.ds(pl.multiple_of(i * 256, 256), 256)] = v[:, seg]

    def before_other():
        for seg in range(4):
            rows_copy(seg).wait_recv()

    def before_edges():
        for slot in range(2):
            edge_copy(0, slot).wait_recv()

    def before_gates():
        for by in (1, 2, 3):
            small_copy(by).wait_recv()
        positions()

    def before_result():
        for m in (1, 0):
            with jax.named_scope(f"swap_{m}"):
                swap(m).wait_recv()
        for colour in range(3):
            for r in range(4):
                with jax.named_scope(f"pass_{colour}_{r}"):
                    message((3, colour, 3, "pass", 0, r)).wait_recv()

    def after_own():
        for by in (1, 2, 3):
            go(small_copy, by)

    def last_states():
        entering()
        states()

    def await_local():
        for copy in local[14:]:
            copy.wait()

    stages = {
        "norm_own": (await_local, lambda i: norm_unit(c, i), after_own),
        "norm_other": (before_other, lambda i: norm_unit(1 - c, i), None),
        "norm_edges": (before_edges, lambda i: norm_edges(), None),
        "source": (None, source, None),
        "source_edges": (None, lambda i: source_edges(), None),
        "gates": (before_gates, gates, None),
        "totals": (None, lambda i: totals(), lambda: tell(0)),
        "hear0": (None, lambda i: hear(0), None),
        "hear1": (None, lambda i: hear(1), None),
        "hear2": (None, lambda i: hear(2), None),
        "shake": (None, shake, None),
        "shake_edges": (None, lambda i: shake_edges(), None),
        "exit_gate": (None, exit_gate, None),
        "conv": (None, conv, lambda: go(swap, 1)),
        "states": (None, lambda i: last_states(), lambda: go(swap, 0)),
        "result": (before_result, result, None),
    }
    held = {0: local[0:3], 1: local[3:5], 2: local[5:7], 3: out_local}
    units = {name: count for name, count, _, _ in STAGES}

    def follow(step):
        if step[0] == "send":
            for copy in held.pop(step[1][0], ()):
                copy.wait()
            go(message, step[1])
        elif step[0] == "wait":
            if step[1][2] < 3:
                group_here(step[1])
        else:
            stages[step[1]][1](0)

    order, _ = plan()
    n = 0
    while n < len(order):
        step = order[n]
        if step[0] != "unit" or units[step[1]] == 1:
            if step[0] == "unit":
                before, work, after = stages[step[1]]
                with jax.named_scope(step[1]):
                    if before is not None:
                        before()
                    work(0)
                    if after is not None:
                        after()
            else:
                with jax.named_scope("_".join(str(v) for v in (step[0],) + step[1])):
                    follow(step)
            n += 1
            continue
        name = step[1]
        count = units[name]
        between = {}
        i = 0
        n += 1
        while i + 1 < count:
            if order[n] == ("unit", name, i + 1):
                i += 1
            else:
                between.setdefault(i, []).append(order[n])
            n += 1
        before, work, after = stages[name]
        with jax.named_scope(name):
            if before is not None:
                before()

            def one(k, _):
                with jax.named_scope("unit"):
                    work(k)
                for at, todo in between.items():

                    @pl.when(k == at)
                    def _():
                        for item in todo:
                            with jax.named_scope("_".join(str(v) for v in ((item[0],) + item[1] if item[0] != "unit" else item))):
                                follow(item)

                return 0

            lax.fori_loop(0, count, one, 0)
            if after is not None:
                after()
    with jax.named_scope("drain"):
        for n in range(max(0, len(sends) - POOL), len(sends)):
            finish(n)


def body(
    activation_sequence,
    rms_multiplier_vector,
    linear_memory_source_matrix,
    linear_memory_exit_matrix,
    filter_exit_mask_matrix,
    filter_entry_mask_matrix,
    filter_source_matrix,
    memory_prefilter_taps,
    filter_taps_depthwise,
    fading_mask_diagonal_tiles,
    entry_mask_diagonal_tiles,
    fading_speed_per_channel,
    speed_multiplier,
    jump_per_position,
    boundary_hidden_vectors,
    final_mixing_matrix,
):
    dma = pltpu.SemaphoreType.DMA
    mixed = pl.pallas_call(
        kernel,
        name="layer",
        out_shape=jax.ShapeDtypeStruct((256, 2, WIDE), bf16),
        in_specs=[pl.BlockSpec(memory_space=pl.ANY)] * 16,
        out_specs=pl.BlockSpec(memory_space=pltpu.VMEM),
        scratch_shapes=[
            pltpu.VMEM((2, STEPS, 4, 2, WIDE), bf16),
            pltpu.VMEM((4, 2, WIDE), bf16),
            pltpu.VMEM((2 * OWN + 32, WIDE), bf16),
            pltpu.VMEM((4, 4, 4, W_END, LANES), bf16),
            pltpu.VMEM((4, 4, 4, 2, OUT_ROWS, LANES), bf16),
            pltpu.VMEM((16, LANES), bf16),
            pltpu.VMEM((4, LANES), bf16),
            pltpu.VMEM((3, LANES), bf16),
            pltpu.VMEM((2, LANES), f32),
            pltpu.VMEM((2, 2, LANES), f32),
            pltpu.VMEM((2, 16, LANES), f32),
            pltpu.VMEM((4, 16, LANES), f32),
            pltpu.VMEM((2, 1024, LANES), f32),
            pltpu.VMEM((2, 2, 544, 256), f32),
            pltpu.VMEM((2, 2, 544, 256), f32),
            pltpu.VMEM((2, 32, 256), f32),
            pltpu.VMEM((2, 2, 2, OWN, 256), f32),
            pltpu.VMEM((2, 2, 2, OWN, 256), f32),
            pltpu.VMEM((2, 2, OWN, 256), f32),
            pltpu.VMEM((2, 2, 4, OWN, LANES), bf16),
            pltpu.VMEM((2, 4, OWN, LANES), bf16),
            pltpu.VMEM((2, 2, 2, 2, 8, 256), f32),
            pltpu.VMEM((3, 2, 2, 2, 8, 256), f32),
            pltpu.VMEM((3, 4, 8, 512), f32),
            dma((18,)),
            dma((16,)),
            dma((POOL,)),
            dma((204,)),
            dma((3, 4)),
            dma((4,)),
            dma((2,)),
            dma((3,)),
            dma((9,)),
            dma((2,)),
        ],
        compiler_params=pltpu.CompilerParams(
            collective_id=0, has_side_effects=True, vmem_limit_bytes=54 * 1024 * 1024
        ),
    )(
        activation_sequence,
        rms_multiplier_vector.reshape(16, LANES),
        linear_memory_source_matrix,
        linear_memory_exit_matrix,
        filter_exit_mask_matrix,
        filter_entry_mask_matrix,
        filter_source_matrix,
        memory_prefilter_taps,
        filter_taps_depthwise,
        fading_mask_diagonal_tiles.reshape(256, LANES),
        entry_mask_diagonal_tiles.reshape(256, LANES),
        fading_speed_per_channel,
        speed_multiplier.reshape(16, LANES),
        jump_per_position.reshape(16, LANES),
        boundary_hidden_vectors,
        final_mixing_matrix.transpose(0, 2, 1),
    )
    return pl.pallas_call(
        hand_over,
        name="hand_over",
        out_shape=jax.ShapeDtypeStruct(mixed.shape, bf16),
        in_specs=[pl.BlockSpec(memory_space=pl.ANY)],
        out_specs=pl.BlockSpec(memory_space=pl.ANY),
        scratch_shapes=[pltpu.VMEM((256, 2, WIDE), bf16), dma((8,)), dma((8,))],
    )(mixed)


def hand_over(src, dst, held, in_sem, out_sem):
    parts = [pl.ds(n * 32, 32) for n in range(8)]
    reads = [pltpu.make_async_copy(src.at[p], held.at[p], in_sem.at[n]) for n, p in enumerate(parts)]
    writes = [pltpu.make_async_copy(held.at[p], dst.at[p], out_sem.at[n]) for n, p in enumerate(parts)]
    for copy in reads:
        copy.start()
    for a, b in zip(reads, writes):
        a.wait()
        b.start()
    for copy in writes:
        copy.wait()


def solution(mesh):
    return jax.shard_map(
        body,
        mesh=mesh,
        in_specs=(
            P(("sp", "tp"), None, None),
            P(),
            P("sp", "tp"),
            P("sp", "tp"),
            P("sp", "tp"),
            P("sp", "tp"),
            P("sp", "tp"),
            P(None, "tp"),
            P(None, "tp"),
            P(None, "tp", None, None),
            P(None, "tp", None, None),
            P(None, "tp"),
            P("sp"),
            P("sp"),
            P(None, None, "tp"),
            P(None, None, ("sp", "tp")),
        ),
        out_specs=P(("sp", "tp"), None, None),
        check_vma=False,
    )
```

time: 745 us -> 91.1 us (0.12); the launches traced: 734 us -> 91 us
  local copies, waits for them, and re-layouts: 328 us -> 0 us
  waiting for transfers between devices: 249 us -> 0 us
  Pallas kernels: 0 us -> 91 us
  other arithmetic: 75.3 us -> 0 us
  matrix products: 34.8 us -> 0 us
  starting transfers between devices: 28.3 us -> 0 us
  between operations: 17.7 us -> 0.01 us
    slice x163 -> x0, local copies, waits for them, and re-layouts: 181 us -> none  [the longest x158 181 us: body(): lax.associative_scan(combine, (decay, drive), axis=0, reverse=scan_direct...]
    reduce_scatter x1 -> x0, waiting for transfers between devices: 172 us -> none  [body(): lax.psum_scatter(jnp.einsum('klbc,kcd->lbd', part_rows, own_weight, prefe...]
    pallas_call x0 -> x2, Pallas kernels: none -> 91 us  [the longest x1 88.6 us: body(): pl.pallas_call(kernel, name='layer', out_shape=jax.ShapeDtypeStruct((256,...]
    pad x80 -> x0, local copies, waits for them, and re-layouts: 60.5 us -> none  [body(): lax.associative_scan(combine, (decay, drive), axis=0, reverse=scan_direct...]
    all_gather x3 -> x0, waiting for transfers between devices: 37.9 us -> none  [the longest x2 37.9 us: on_gathered_pieces(): parts = [lax.all_gather(share, axis) for share in pieces]]
    all_to_all x3 -> x0, waiting for transfers between devices: 37.4 us -> none  [the longest x2 37.4 us: sent_to_all(): return lax.all_to_all(copies, axis, split_axis=0, concat_axis=0, tiled=True)]
    dot_general x5 -> x0, matrix products: 34.8 us -> none  [the longest x2 19.8 us: project(): jnp.dot(piece, in_weights, preferred_element_type=jnp.float32)]
    add x118 -> x0, other arithmetic: 33.8 us -> none  [the longest x46 22.6 us: body(): lax.associative_scan(combine, (decay, drive), axis=0, reverse=scan_direct...]
  transfers between devices with their start and end apart: 9 -> 0, of which waited for: 4 -> 0; matrix products, arithmetic and copies ran while one was open for 54% -> 0% of each run, Pallas kernels for 0% -> 0%
where the time goes in v1:
time: 91.1 us; the launch traced here: 91 us
  Pallas kernels  91 us (100%)
    pallas_call x1, Pallas kernels, body(): pl.pallas_call(kernel, name='layer', out_shape=jax.ShapeDtypeStruct((256,...  88.6 us
    pallas_call x1, Pallas kernels, body(): pl.pallas_call(hand_over, name='hand_over', out_shape=jax.ShapeDtypeStruc...  2.39 us

profile of v1, /device:TPU:1, one launch (start us, length us, event | category | flops | bytes accessed | tf_op | source)
XLA Modules:
  0.0 91.0 jit_solution(14756660938963928816)
XLA Ops:
  0.0 88.6 %layer.1.src = bf16[256,2,2048]{2,1,0:T(2,128)(2,1)} custom-call(bf16[256,2,2048]{2,1,0:T(2,128)(2,1)} %x_in.1, bf16[16,128]{1,0:T(8,128)(2,1)} %bitcast.11, bf16[128,128]{1,0:T(8,128)(2,1)} %src_in.1, bf16[128,128]{1,0:T(8,128)(2,1)} %exit_in.1, bf16[128,128]{1,0:T(8,128)(2,1)} %cout_in.1, bf16[128,128]{1,0:T(8,128)(2,1)} %cgate_in.1, ...), custom_call_target="tpu_custom_call" | custom-call | tf_op jit(solution)/shard_map/layer/pallas_call | solution.py:830
  88.6 2.4 %hand_over.1 = bf16[256,2,2048]{2,1,0:T(2,128)(2,1)} custom-call(bf16[256,2,2048]{2,1,0:T(2,128)(2,1)} %layer.1.src), custom_call_target="tpu_custom_call" | custom-call | tf_op jit(solution)/shard_map/hand_over/pallas_call | solution.py:893

commit v2 on v1

--- a/solution.py
+++ b/solution.py
@@ -25,6 +25,8 @@
     ("w", ((416, 496), (496, 592), (592, 672))),
     ("o", ((0, 80), (80, 160), (160, 256))),
 )
+FINE = (True, True, True, True)
+FAR = ()
 ORDERS = (("y", "x", "z"), ("x", "z", "y"), ("z", "y", "x"))
 NEAR = (0, -1, 1, 2)
 FORWARD = {1: (0, -1), -1: (1, 2)}
@@ -34,15 +36,25 @@
     return 1 if piece % 2 == 0 else -1
 
 
+def places(piece):
+    return 7 if FINE[piece] else 5
+
+
+def first_place(piece, colour):
+    return sum(3 * (3 + 2 * places(p)) for p in range(piece)) + colour * (3 + 2 * places(piece))
+
+
 def group_of(m):
     piece, colour, phase, kind, way, r = m
     if kind == "pass":
-        return (piece, colour, 3, r, 1)
+        return (piece, colour, 3, 0, 4)
     if phase == 0:
-        return (piece, colour, 0, 2 if kind == "fwd" else (0 if way == 1 else 1), 1)
-    first = 3 + 7 * (phase - 1)
-    if kind == "fwd":
-        return (piece, colour, phase, first + 6, 4)
+        return (piece, colour, 0, 2 if kind != "own" else (0 if way == 1 else 1), 1)
+    first = 3 + places(piece) * (phase - 1)
+    if kind != "own":
+        return (piece, colour, phase, first + places(piece) - 1, 4 if FINE[piece] else 2)
+    if not FINE[piece]:
+        return (piece, colour, phase, first + (r if way == 1 else 3 - r), 1)
     alone = FORWARD[way]
     place = alone.index(r) if r in alone else 2
     return (piece, colour, phase, first + place + (0 if way == 1 else 3), 1 if r in alone else 2)
@@ -51,68 +63,86 @@
 def messages(piece, colour):
     found = {}
     up = turn_of(piece)
-
-    def own(phase, way, r):
-        return (piece, colour, phase, "own", way, r)
-
-    def fwd(phase, way, r):
-        return (piece, colour, phase, "fwd", way, r)
+    fine = FINE[piece]
+
+    def one(phase, kind, way, r):
+        return (piece, colour, phase, kind, way, r)
 
     def here(*given):
         return tuple(dict.fromkeys(group_of(m) for m in given))
 
-    ready = {-1: here(own(0, 1, 0)), 1: here(own(0, -1, 0)), 2: here(fwd(0, up, 0)), 0: ()}
-    first = here(own(0, 1, 0), own(0, -1, 0), fwd(0, up, 0))
-    for way in (1, -1):
-        found[own(0, way, 0)] = ()
-    found[fwd(0, up, 0)] = here(own(0, up, 0))
+    def both(phase, r, needs):
+        for way in (1, -1):
+            found[one(phase, "own", way, r)] = needs
+
+    both(0, 0, ())
+    if (piece, 0) in FAR:
+        opposite = one(0, "far", up, 0)
+        found[opposite] = ()
+    else:
+        opposite = one(0, "fwd", up, 0)
+        found[opposite] = here(one(0, "own", up, 0))
+    near = [one(0, "own", 1, 0), one(0, "own", -1, 0)]
+    before = here(*near, opposite)
+    ready = {0: (), -1: here(near[0]), 1: here(near[1]), 2: here(opposite)}
     for phase in (1, 2):
-        for r in NEAR:
+        for r in NEAR if fine else (0, 1):
+            both(phase, r, ready[r] if fine else before)
+        last = []
+        if (piece, phase) in FAR:
+            for r in NEAR:
+                last.append(one(phase, "far", up, r))
+                found[last[-1]] = ready[r]
+        else:
             for way in (1, -1):
-                found[own(phase, way, r)] = ready[r]
-        for way in (1, -1):
-            for r in FORWARD[way]:
-                found[fwd(phase, way, r)] = here(own(phase, way, r))
+                for r in FORWARD[way] if fine else ((0,) if way == 1 else (1,)):
+                    last.append(one(phase, "fwd", way, r))
+                    found[last[-1]] = here(one(phase, "own", way, r))
+        parts = NEAR if fine else (0, 1)
         ready = {
-            0: first,
-            -1: here(*(own(phase, 1, r) for r in NEAR)),
-            1: here(*(own(phase, -1, r) for r in NEAR)),
-            2: here(fwd(phase, 1, 0)),
+            0: before,
+            -1: here(*(one(phase, "own", 1, r) for r in parts)),
+            1: here(*(one(phase, "own", -1, r) for r in parts)),
+            2: here(*last),
         }
-    if piece == 3:
-        before = here(*(m for m in found if m[2] < 2))
-        for slot, r in enumerate((0, -1, 1, 2)):
-            found[(piece, colour, 3, "pass", 0, slot)] = before if r == 0 else ready[r]
+        if phase == 2:
+            break
+        before = before + ready[-1] + ready[1] + ready[2]
+    if PIECES[piece][0] == "o":
+        for slot, r in enumerate(NEAR):
+            found[one(3, "pass", 0, slot)] = before if r == 0 else ready[r]
     return found
 
 
 def size(m):
     first, last = PIECES[m[0]][1][m[1]]
-    return (last - first) * 0.25 * (1, 1, 4, 16)[m[2]]
-
-
-RATE, HOP = 44.0, 2.2
+    chunks = (1, 1, 4, 16)[m[2]] * (1 if FINE[m[0]] or m[2] in (0, 3) else 2)
+    return (last - first) * 0.25 * chunks * (2 if m[3] == "far" else 1)
+
+
+RATE, HOP = 44.0, 2.8
 SIDE_RATE, SIDE_HOP = 450.0, 1.4
 
 STAGES = (
-    ("norm_own", 4, 1.5, ()),
-    ("norm_other", 4, 1.5, ("rows",)),
+    ("norm_own", 4, 1.55, ()),
+    ("norm_other", 4, 1.55, ("rows",)),
     ("norm_edges", 1, 0.3, ("edges",)),
-    ("source", 4, 0.8, ("norm_own", "norm_other", "norm_edges", 0)),
+    ("spots", 1, 0.8, ("small",)),
+    ("source", 4, 0.78, ("norm_own", "norm_other", "norm_edges", 0)),
     ("source_edges", 1, 0.6, ("source",)),
-    ("gates", 4, 1.95, ("source_edges", "small")),
-    ("totals", 1, 1.3, ("gates",)),
+    ("gates", 2, 1.65, ("source_edges", "spots")),
+    ("gates_shake", 4, 1.85, ("gates", 1)),
+    ("totals", 1, 1.3, ("gates_shake",)),
     ("hear0", 1, 0.4, ("told0",)),
     ("hear1", 1, 0.4, ("told1",)),
     ("hear2", 1, 0.5, ("told2",)),
-    ("shake", 4, 1.4, ("norm_own", "norm_other", "norm_edges", 1)),
-    ("shake_edges", 1, 0.8, ("shake",)),
-    ("exit_gate", 4, 0.78, (2, "norm_other")),
-    ("conv", 4, 0.75, (2, "shake_edges")),
+    ("shake_edges", 1, 0.8, ("gates_shake",)),
+    ("exit_gate", 4, 0.8, (2, "norm_other")),
+    ("conv", 4, 0.8, (2, "shake_edges")),
     ("states", 1, 1.5, ("hear2", "exit_gate")),
-    ("result", 8, 0.85, (3, "swapped0", "swapped1")),
+    ("result", 8, 0.78, (3, "swapped0", "swapped1")),
 )
-BACKLOG = 1.0
+BACKLOG = 1.5
 
 
 def PRIORITY(m):
@@ -121,7 +151,7 @@
 
 def plan():
     deps = {}
-    for piece in range(4):
+    for piece in range(len(PIECES)):
         for colour in range(3):
             deps.update(messages(piece, colour))
     groups = {}
@@ -139,7 +169,7 @@
             if link.get(wire, 0.0) - clock > BACKLOG:
                 continue
             link[wire] = max(clock, link.get(wire, 0.0)) + size(m) / (SIDE_RATE if side else RATE)
-            arrive[m] = link[wire] + (SIDE_HOP if side else HOP)
+            arrive[m] = link[wire] + (SIDE_HOP if side else HOP + (0.8 if m[3] == "far" else 0.0))
             sent.add(m)
             order.append(("send", m))
             g = group_of(m)
@@ -227,8 +257,8 @@
 def kernel(
     x_in, gain_in, src_in, exit_in, cout_in, cgate_in, cin_in, taps_in, ctaps_in, fade_in, entry_in, speed_in,
     tempo_in, jump_in, edge_in, out_w, out,
-    XR, XE, X, G, Wo, GN, TB, CB, SB, BB, PM, SM, MJ, Rp, Sp, Hh, A, U, GL, ACT, ACTS, SEG, PRE, XS,
-    lsem, wsem, pool, grecv, frecv, xrecv, hrecv, srecv, erecv, arecv,
+    XR, XE, X, G, Wo, GN, TB, CB, SB, BB, PM, SM, MJ, Rp, Sp, Hh, A, U, GL, ACT, ACTS, SEG, PRE, XS, OUT,
+    lsem, wsem, pool, grecv, frecv, xrecv, hrecv, srecv, erecv, arecv, osem,
 ):
     sp, tp = lax.axis_index("sp"), lax.axis_index("tp")
     me = {"z": sp // 4, "x": lax.rem(sp, 4), "y": tp // 2}
@@ -323,11 +353,6 @@
             x_in.at[pl.ds(c * 254, 2)], XE.at[pl.ds((1 - c) * 2, 2)], send, hrecv.at[slot], chip(target, core)
         )
 
-    for seg in range(4):
-        go(rows_copy, seg)
-    for core in range(2):
-        go(edge_copy, core, 1 - c)
-
     def region(piece, colour, phase, i, r, count=1):
         kind, parts = PIECES[piece]
         first, last = parts[colour]
@@ -335,14 +360,18 @@
         where = dict(me)
         if phase == 0:
             where[a] = i
-        elif phase == 1:
-            where[a], where[b] = wrap(me[a] + r), i
+        elif phase < 3:
+            cut = (a, b)[phase - 1]
+            if phase == 2:
+                where[a] = slice(None)
+            where[(b, d)[phase - 1]] = i
+            if FINE[piece]:
+                where[cut] = wrap(me[cut] + r) if count == 1 else pl.ds(0, count)
+            else:
+                where[cut] = pl.ds(2 * r, 2) if count == 1 else slice(None)
         else:
-            where[a], where[b], where[d] = slice(None), wrap(me[b] + r), i
-            if phase == 3:
-                where[b] = slice(None)
-        if count > 1:
-            where[(a, b)[phase - 1]] = pl.ds(0, count)
+            where[a], where[b] = slice(None), slice(None)
+            where[d] = i if count == 1 else slice(None)
         rows = pl.ds(first, last - first)
         if kind == "w":
             return G.at[where["z"], where["x"], where["y"], rows]
@@ -352,29 +381,32 @@
         piece, colour, phase, kind, way, r = m
         if kind == "pass":
             d = ORDERS[colour][2]
-            ref = region(piece, colour, 3, wrap(me[d] + (0, -1, 1, 2)[r]), 0)
-            return remote(ref, ref, send, frecv.at[colour, r], sibling)
+            ref = region(piece, colour, 3, wrap(me[d] + NEAR[r]), 0)
+            return remote(ref, ref, send, frecv.at[(piece - 3) * 3 + colour], sibling)
         d = ORDERS[colour][phase]
-        block = me[d] if kind == "own" else wrap(me[d] - way)
+        block = wrap(me[d] - way) if kind == "fwd" else me[d]
         ref = region(piece, colour, phase, block, r)
-        return remote(ref, ref, send, grecv.at[(piece * 3 + colour) * 17 + group_of(m)[3]], device(along(d, way), c))
+        at = first_place(piece, colour) + group_of(m)[3]
+        return remote(ref, ref, send, grecv.at[at], device(along(d, 2 if kind == "far" else way), c))
 
     def group_here(g):
         piece, colour, phase, place, count = g
         ref = region(piece, colour, phase, 0, 0, count)
-        remote(ref, ref, None, grecv.at[(piece * 3 + colour) * 17 + place], sibling).wait_recv()
-
-    for copy in local[7:14]:
-        copy.wait()
-    for row in range(4):
-        SM[y, row : row + 1, :] = TB[row : row + 1, :].astype(f32)
-    for row in range(3):
-        SM[y, 4 + row : 5 + row, :] = CB[row : row + 1, :].astype(f32)
-    for row in range(2):
-        SM[y, 7 + row : 8 + row, :] = SB[row : row + 1, :]
-        for b in range(2):
-            SM[y, 9 + 2 * row + b : 10 + 2 * row + b, :] = BB[row, b : b + 1, :]
-    SM[y, 13:16, :] = jnp.zeros((3, LANES), f32)
+        at = frecv.at[(piece - 3) * 3 + colour] if phase == 3 else grecv.at[first_place(piece, colour) + place]
+        remote(ref, ref, None, at, sibling).wait_recv()
+
+    def small_arrays():
+        for copy in local[7:14]:
+            copy.wait()
+        for row in range(4):
+            SM[y, row : row + 1, :] = TB[row : row + 1, :].astype(f32)
+        for row in range(3):
+            SM[y, 4 + row : 5 + row, :] = CB[row : row + 1, :].astype(f32)
+        for row in range(2):
+            SM[y, 7 + row : 8 + row, :] = SB[row : row + 1, :]
+            for b in range(2):
+                SM[y, 9 + 2 * row + b : 10 + 2 * row + b, :] = BB[row, b : b + 1, :]
+        SM[y, 13:16, :] = jnp.zeros((3, LANES), f32)
 
     def small_copy(by, send=None):
         return remote(SM.at[y], SM.at[y], send, srecv.at[by - 1], device(along("y", by), c))
@@ -472,41 +504,40 @@
 
     def gates(i):
         def one(k, _):
-            gate_rows(i // 2, lax.rem(i, 2), k)
+            gate_rows(0, i, k)
             return 0
 
         lax.fori_loop(0, 4, one, 0)
 
     def gate_rows(yp, rc, blk):
         base = pl.multiple_of(blk * GB, GB)
-        rc_rows = jnp.zeros((GB, 256), f32)
-        for k in range(4):
+        rc_rows = taps(yp, 0) * Rp[yp, rc, pl.ds(base, GB), :]
+        for k in range(1, 4):
             rc_rows = rc_rows + taps(yp, k) * Rp[yp, rc, pl.ds(base + 8 * k, GB), :]
-        narrow = rc_rows.astype(bf16)
-        wide = narrow.astype(f32)
+        narrow = (0.5 * rc_rows).astype(bf16)
+        half = narrow.astype(f32)
         at = pl.ds(pl.multiple_of(rc * OWN + blk * GB, GB), GB)
         tempo, jump = MJ[0, at, :], MJ[1, at, :]
         for h in range(2):
             lane = slice(h * LANES, (h + 1) * LANES)
             yy = 2 * yp + h
             maps = [
-                    G[pl.ds(2 * d, 2), :, yy, pl.ds(GATES + 16 * kind, 16), :].reshape(LANES, LANES)
-                    for kind in range(2)
-                    for d in range(2)
-                ]
+                G[pl.ds(2 * d, 2), :, yy, pl.ds(GATES + 16 * kind, 16), :].reshape(LANES, LANES)
+                for kind in range(2)
+                for d in range(2)
+            ]
             for d in range(2):
                 pre = jnp.dot(
                     narrow[:, lane], jnp.concatenate([maps[d], maps[2 + d]], axis=1), preferred_element_type=f32
                 )
                 speed = SM[yy, pl.ds(7 + d, 1), :] * -4.0
-                la = (1.0 + jnp.tanh(0.5 * pre[:, :LANES])) * (speed * tempo) + jump
+                la = (1.0 + jnp.tanh(pre[:, :LANES])) * (speed * tempo) + jump
                 decay = jnp.exp(la)
-                t = 2.0 * la
-                near = -t * (1.0 + t * (0.5 + t * (1.0 / 6.0 + t * (1.0 / 24.0 + t * (1.0 / 120.0)))))
-                rest = jnp.where(t > -0.1, near, 1.0 - decay * decay)
-                opening = 0.5 + 0.5 * jnp.tanh(0.5 * pre[:, LANES:])
+                near = la * (-2.0 - la * (2.0 + la * (4.0 / 3.0)))
+                rest = jnp.where(la > -0.005, near, 1.0 - decay * decay)
+                root = rest * lax.rsqrt(jnp.maximum(rest, 1e-36))
                 A[d, yp, rc, pl.ds(base, GB), lane] = decay
-                U[d, yp, rc, pl.ds(base, GB), lane] = jnp.sqrt(rest) * opening * wide[:, lane]
+                U[d, yp, rc, pl.ds(base, GB), lane] = root * (1.0 + jnp.tanh(pre[:, LANES:])) * half[:, lane]
 
     PAIRS = [(yp, rc) for yp in range(2) for rc in range(2)]
 
@@ -649,6 +680,11 @@
 
         block(work, i)
 
+    def gates_shake(i):
+        shake(i)
+        for k in range(2):
+            gate_rows(1, i // 2, lax.rem(i, 2) * 2 + k)
+
     def shake_edges():
         for yp in range(2):
             Hh[yp] = project(edges, weight(CGATE, yp)) * project(edges, weight(CIN, yp))
@@ -683,9 +719,16 @@
             jnp.concatenate(left, axis=1), jnp.concatenate(right, axis=1),
             (((1,), (1,)), ((), ())), preferred_element_type=f32,
         )
-        v = v.astype(bf16).reshape(STEPS, 4, 2, 256)
-        for seg in range(4):
-            out[seg * STEPS : (seg + 1) * STEPS, :, pl.ds(pl.multiple_of(i * 256, 256), 256)] = v[:, seg]
+        OUT[:, :, :, pl.ds(pl.multiple_of(i * 256, 256), 256)] = v.astype(bf16).reshape(STEPS, 4, 2, 256)
+
+        @pl.when(lax.rem(i, 4) == 3)
+        def _():
+            for seg in range(4):
+                write(i // 4, seg).start()
+
+    def write(i, seg):
+        lanes = pl.ds(pl.multiple_of(i * 1024, 1024), 1024)
+        return pltpu.make_async_copy(OUT.at[:, seg, :, lanes], out.at[pl.ds(seg * STEPS, STEPS), :, lanes], osem.at[i, seg])
 
     def before_other():
         for seg in range(4):
@@ -702,12 +745,7 @@
 
     def before_result():
         for m in (1, 0):
-            with jax.named_scope(f"swap_{m}"):
-                swap(m).wait_recv()
-        for colour in range(3):
-            for r in range(4):
-                with jax.named_scope(f"pass_{colour}_{r}"):
-                    message((3, colour, 3, "pass", 0, r)).wait_recv()
+            swap(m).wait_recv()
 
     def after_own():
         for by in (1, 2, 3):
@@ -718,6 +756,11 @@
         states()
 
     def await_local():
+        for seg in range(4):
+            go(rows_copy, seg)
+        for core in range(2):
+            go(edge_copy, core, 1 - c)
+        small_arrays()
         for copy in local[14:]:
             copy.wait()
 
@@ -727,12 +770,13 @@
         "norm_edges": (before_edges, lambda i: norm_edges(), None),
         "source": (None, source, None),
         "source_edges": (None, lambda i: source_edges(), None),
-        "gates": (before_gates, gates, None),
+        "spots": (None, lambda i: before_gates(), None),
+        "gates": (None, gates, None),
+        "gates_shake": (None, gates_shake, None),
         "totals": (None, lambda i: totals(), lambda: tell(0)),
         "hear0": (None, lambda i: hear(0), None),
         "hear1": (None, lambda i: hear(1), None),
         "hear2": (None, lambda i: hear(2), None),
-        "shake": (None, shake, None),
         "shake_edges": (None, lambda i: shake_edges(), None),
         "exit_gate": (None, exit_gate, None),
         "conv": (None, conv, lambda: go(swap, 1)),
@@ -748,8 +792,7 @@
                 copy.wait()
             go(message, step[1])
         elif step[0] == "wait":
-            if step[1][2] < 3:
-                group_here(step[1])
+            group_here(step[1])
         else:
             stages[step[1]][1](0)
 
@@ -803,6 +846,9 @@
             lax.fori_loop(0, count, one, 0)
             if after is not None:
                 after()
+    for i in range(2):
+        for seg in range(4):
+            write(i, seg).wait()
     with jax.named_scope("drain"):
         for n in range(max(0, len(sends) - POOL), len(sends)):
             finish(n)
@@ -832,7 +878,7 @@
         name="layer",
         out_shape=jax.ShapeDtypeStruct((256, 2, WIDE), bf16),
         in_specs=[pl.BlockSpec(memory_space=pl.ANY)] * 16,
-        out_specs=pl.BlockSpec(memory_space=pltpu.VMEM),
+        out_specs=pl.BlockSpec(memory_space=pl.ANY),
         scratch_shapes=[
             pltpu.VMEM((2, STEPS, 4, 2, WIDE), bf16),
             pltpu.VMEM((4, 2, WIDE), bf16),
@@ -858,16 +904,18 @@
             pltpu.VMEM((2, 2, 2, 2, 8, 256), f32),
             pltpu.VMEM((3, 2, 2, 2, 8, 256), f32),
             pltpu.VMEM((3, 4, 8, 512), f32),
+            pltpu.VMEM((STEPS, 4, 2, WIDE), bf16),
             dma((18,)),
             dma((16,)),
             dma((POOL,)),
-            dma((204,)),
-            dma((3, 4)),
+            dma((first_place(len(PIECES) - 1, 3),)),
+            dma((3,)),
             dma((4,)),
             dma((2,)),
             dma((3,)),
             dma((9,)),
             dma((2,)),
+            dma((2, 4)),
         ],
         compiler_params=pltpu.CompilerParams(
             collective_id=0, has_side_effects=True, vmem_limit_bytes=54 * 1024 * 1024

time: 91.1 us -> 86.2 us (0.946)
  Pallas kernels: 91 us -> 86.1 us
    pallas_call x1, Pallas kernels: 88.6 us -> 83.7 us  [body(): pl.pallas_call(kernel, name='layer', out_shape=jax.ShapeDtypeStruct((256,...]
where the time goes in v2:
time: 86.2 us; the launch traced here: 86.1 us
  Pallas kernels  86.1 us (100%)
    pallas_call x1, Pallas kernels, body(): pl.pallas_call(kernel, name='layer', out_shape=jax.ShapeDtypeStruct((256,...  83.7 us
    pallas_call x1, Pallas kernels, body(): pl.pallas_call(hand_over, name='hand_over', out_shape=jax.ShapeDtypeStruc...  2.39 us

profile of v2, /device:TPU:1, one launch (start us, length us, event | category | flops | bytes accessed | tf_op | source)
XLA Modules:
  0.0 86.1 jit_solution(9454481055586687494)
XLA Ops:
  0.0 83.7 %layer.1.src = bf16[256,2,2048]{2,1,0:T(2,128)(2,1)} custom-call(bf16[256,2,2048]{2,1,0:T(2,128)(2,1)} %x_in.1, bf16[16,128]{1,0:T(8,128)(2,1)} %bitcast.11, bf16[128,128]{1,0:T(8,128)(2,1)} %src_in.1, bf16[128,128]{1,0:T(8,128)(2,1)} %exit_in.1, bf16[128,128]{1,0:T(8,128)(2,1)} %cout_in.1, bf16[128,128]{1,0:T(8,128)(2,1)} %cgate_in.1, ...), custom_call_target="tpu_custom_call" | custom-call | tf_op jit(solution)/shard_map/layer/pallas_call | solution.py:876
  83.7 2.4 %hand_over.1 = bf16[256,2,2048]{2,1,0:T(2,128)(2,1)} custom-call(bf16[256,2,2048]{2,1,0:T(2,128)(2,1)} %layer.1.src), custom_call_target="tpu_custom_call" | custom-call | tf_op jit(solution)/shard_map/hand_over/pallas_call | solution.py:941

commit v3 on v2

--- a/solution.py
+++ b/solution.py
@@ -14,7 +14,7 @@
 STEPS = 64
 WIDE = 2048
 LANES = 128
-POOL = 32
+POOL = 48
 
 SRC, GATES, CGATE, CIN, COUT, EXIT, W_END = 0, 128, 160, 288, 416, 544, 672
 OUT_ROWS = 256
@@ -137,10 +137,10 @@
     ("hear1", 1, 0.4, ("told1",)),
     ("hear2", 1, 0.5, ("told2",)),
     ("shake_edges", 1, 0.8, ("gates_shake",)),
-    ("exit_gate", 4, 0.8, (2, "norm_other")),
-    ("conv", 4, 0.8, (2, "shake_edges")),
+    ("exit_gate", 2, 1.5, (2, "norm_other")),
+    ("conv", 2, 1.5, (2, "shake_edges")),
     ("states", 1, 1.5, ("hear2", "exit_gate")),
-    ("result", 8, 0.78, (3, "swapped0", "swapped1")),
+    ("result", 4, 1.5, (3, "swapped0", "swapped1")),
 )
 BACKLOG = 1.5
 
@@ -467,6 +467,12 @@
     def project(rows, w):
         return jnp.dot(X[rows, :], w, preferred_element_type=f32)
 
+    def wide(work, i):
+        w = jnp.concatenate([G[:, :, y4, pl.ds(work[0], LANES), :].reshape(WIDE, LANES) for y4 in range(4)], axis=1)
+        v = project(pl.ds(pl.multiple_of(i * OWN, OWN), OWN), w)
+        for yp in range(2):
+            work[1](yp, i, v[:, yp * 256 : (yp + 1) * 256])
+
     def block(work, i):
         yp, rc = i // 2, lax.rem(i, 2)
         work(yp, rc, pl.ds(pl.multiple_of(rc * OWN, OWN), OWN))
@@ -641,12 +647,11 @@
                     h = spread(a, last) * h + spread(b, last)
 
     def exit_gate(i):
-        def work(yp, rc, rows):
-            v = project(rows, weight(EXIT, yp))
+        def work(yp, rc, v):
             inner = v * (0.7978845608028654 + 0.035677408136300125 * v * v)
             GL[yp, rc] = 0.5 * v * (1.0 + jnp.tanh(inner))
 
-        block(work, i)
+        wide((EXIT, work), i)
 
     def states():
         def forth(i, state):
@@ -691,8 +696,7 @@
         pads(Sp)
 
     def conv(i):
-        def work(yp, rc, rows):
-            v = project(rows, weight(COUT, yp))
+        def work(yp, rc, v):
             s = jnp.zeros((OWN, 256), f32)
             for k in range(3):
                 s = s + taps(yp, 4 + k) * Sp[yp, rc, pl.ds(8 + 8 * k, OWN), :]
@@ -700,13 +704,13 @@
             for h in range(2):
                 ACT[rc, 1, 2 * yp + h] = done[:, h * LANES : (h + 1) * LANES]
 
-        block(work, i)
+        wide((COUT, work), i)
 
     def swap(m, send=None):
         return remote(ACT.at[1 - c, m], ACTS.at[m], send, arecv.at[m], sibling)
 
     def result(i):
-        zz, xx = i // 2, lax.rem(i, 2) * 2
+        zz = i
         left, right = [], []
         for own in range(2):
             core = c if own == 0 else 1 - c
@@ -714,17 +718,17 @@
                 for yy in range(4):
                     left.append(ACT[c, m, yy] if own == 0 else ACTS[m, yy])
                     k16 = pl.ds(pl.multiple_of((m * 8 + 2 * yy + core) * 16, 16), 16)
-                    right.append(Wo[zz, pl.ds(xx, 2), :, :, k16, :].reshape(256, LANES))
+                    right.append(Wo[zz, :, :, :, k16, :].reshape(512, LANES))
         v = lax.dot_general(
             jnp.concatenate(left, axis=1), jnp.concatenate(right, axis=1),
             (((1,), (1,)), ((), ())), preferred_element_type=f32,
         )
-        OUT[:, :, :, pl.ds(pl.multiple_of(i * 256, 256), 256)] = v.astype(bf16).reshape(STEPS, 4, 2, 256)
-
-        @pl.when(lax.rem(i, 4) == 3)
+        OUT[:, :, :, pl.ds(pl.multiple_of(i * 512, 512), 512)] = v.astype(bf16).reshape(STEPS, 4, 2, 512)
+
+        @pl.when(lax.rem(i, 2) == 1)
         def _():
             for seg in range(4):
-                write(i // 4, seg).start()
+                write(i // 2, seg).start()
 
     def write(i, seg):
         lanes = pl.ds(pl.multiple_of(i * 1024, 1024), 1024)

time: 86.2 us -> 84.8 us (0.984)
  Pallas kernels: 86.1 us -> 84.6 us
    pallas_call x1, Pallas kernels: 83.7 us -> 82.2 us  [body(): pl.pallas_call(kernel, name='layer', out_shape=jax.ShapeDtypeStruct((256,...]
where the time goes in v3:
time: 84.8 us; the launch traced here: 84.6 us
  Pallas kernels  84.6 us (100%)
    pallas_call x1, Pallas kernels, body(): pl.pallas_call(kernel, name='layer', out_shape=jax.ShapeDtypeStruct((256,...  82.2 us
    pallas_call x1, Pallas kernels, body(): pl.pallas_call(hand_over, name='hand_over', out_shape=jax.ShapeDtypeStruc...  2.39 us

profile of v3, /device:TPU:1, one launch (start us, length us, event | category | flops | bytes accessed | tf_op | source)
XLA Modules:
  0.0 84.6 jit_solution(4241621879601983505)
XLA Ops:
  0.0 82.2 %layer.1.src = bf16[256,2,2048]{2,1,0:T(2,128)(2,1)} custom-call(bf16[256,2,2048]{2,1,0:T(2,128)(2,1)} %x_in.1, bf16[16,128]{1,0:T(8,128)(2,1)} %bitcast.11, bf16[128,128]{1,0:T(8,128)(2,1)} %src_in.1, bf16[128,128]{1,0:T(8,128)(2,1)} %exit_in.1, bf16[128,128]{1,0:T(8,128)(2,1)} %cout_in.1, bf16[128,128]{1,0:T(8,128)(2,1)} %cgate_in.1, ...), custom_call_target="tpu_custom_call" | custom-call | tf_op jit(solution)/shard_map/layer/pallas_call | solution.py:880
  82.3 2.4 %hand_over.1 = bf16[256,2,2048]{2,1,0:T(2,128)(2,1)} custom-call(bf16[256,2,2048]{2,1,0:T(2,128)(2,1)} %layer.1.src), custom_call_target="tpu_custom_call" | custom-call | tf_op jit(solution)/shard_map/hand_over/pallas_call | solution.py:945

commit v4 on v3

--- a/solution.py
+++ b/solution.py
@@ -120,12 +120,12 @@
     return (last - first) * 0.25 * chunks * (2 if m[3] == "far" else 1)
 
 
-RATE, HOP = 44.0, 2.8
+RATE, HOP = 47.0, 2.8
 SIDE_RATE, SIDE_HOP = 450.0, 1.4
 
 STAGES = (
-    ("norm_own", 4, 1.55, ()),
-    ("norm_other", 4, 1.55, ("rows",)),
+    ("norm_own", 8, 0.79, ()),
+    ("norm_other", 8, 0.79, ("rows",)),
     ("norm_edges", 1, 0.3, ("edges",)),
     ("spots", 1, 0.8, ("small",)),
     ("source", 4, 0.78, ("norm_own", "norm_other", "norm_edges", 0)),
@@ -440,7 +440,7 @@
 
     def norm_unit(rc, i):
         def one(k, _):
-            j = i * 16 + k * 2
+            j = i * 8 + k * 2
             parts = [
                 XR[rc, pl.ds(j, 2), :, :, n * LANES : (n + 1) * LANES].astype(f32).reshape(16, LANES) for n in range(16)
             ]
@@ -449,7 +449,7 @@
                 X[rows, n * LANES : (n + 1) * LANES] = v.astype(bf16)
             return 0
 
-        lax.fori_loop(0, 8, one, 0)
+        lax.fori_loop(0, 4, one, 0)
 
     def norm_edges():
         row = rows_of((8, 1))

time: 84.8 us -> 84.7 us (level)
  no operation moved by 1% of the time
where the time goes in v4:
time: 84.7 us; the launch traced here: 84.6 us
  Pallas kernels  84.6 us (100%)
    pallas_call x1, Pallas kernels, body(): pl.pallas_call(kernel, name='layer', out_shape=jax.ShapeDtypeStruct((256,...  82.2 us
    pallas_call x1, Pallas kernels, body(): pl.pallas_call(hand_over, name='hand_over', out_shape=jax.ShapeDtypeStruc...  2.39 us

profile of v4, /device:TPU:1, one launch (start us, length us, event | category | flops | bytes accessed | tf_op | source)
XLA Modules:
  0.0 84.6 jit_solution(4943794123140976457)
XLA Ops:
  0.0 82.2 %layer.1.src = bf16[256,2,2048]{2,1,0:T(2,128)(2,1)} custom-call(bf16[256,2,2048]{2,1,0:T(2,128)(2,1)} %x_in.1, bf16[16,128]{1,0:T(8,128)(2,1)} %bitcast.11, bf16[128,128]{1,0:T(8,128)(2,1)} %src_in.1, bf16[128,128]{1,0:T(8,128)(2,1)} %exit_in.1, bf16[128,128]{1,0:T(8,128)(2,1)} %cout_in.1, bf16[128,128]{1,0:T(8,128)(2,1)} %cgate_in.1, ...), custom_call_target="tpu_custom_call" | custom-call | tf_op jit(solution)/shard_map/layer/pallas_call | solution.py:880
  82.2 2.4 %hand_over.1 = bf16[256,2,2048]{2,1,0:T(2,128)(2,1)} custom-call(bf16[256,2,2048]{2,1,0:T(2,128)(2,1)} %layer.1.src), custom_call_target="tpu_custom_call" | custom-call | tf_op jit(solution)/shard_map/hand_over/pallas_call | solution.py:945
